TPU v7x, 512 devices: a whole 4x8x8 slice. The times are simulated.
512 devices in a mesh: kv: 128 (over z, y, core), tp: 4 (over x).
Axes of the slice: x: 4, y: 8, z: 8, core: 2. Of those that a mesh axis runs over, the one named last changes fastest.
Arguments:
- hidden: bfloat16 [128, 4096], P(None, 'tp'), may hold values from -50 to 50
- input_gain: bfloat16 [4096], P('tp'), may hold values from 0.099609375 to 1.8984375
- x_weight: bfloat16 [4096, 8192], P('tp', 'kv'), may hold values from -0.09375 to 0.09375
- z_weight: bfloat16 [4096, 8192], P('tp', 'kv'), may hold values from -0.09375 to 0.09375
- bc_weight: bfloat16 [4096, 8192], P('tp', 'kv'), may hold values from -0.09375 to 0.09375
- dt_weight: bfloat16 [4096, 128], P('tp', 'kv'), may hold values from -0.09375 to 0.09375
- x_kernel: bfloat16 [4, 8192], P(None, 'kv'), may hold values from -3 to 3
- bc_kernel: bfloat16 [4, 8192], P(None, 'kv'), may hold values from -3 to 3
- dt_bias: float32 [128], P('kv'), may hold values from -3 to 0.5
- decay_log: float32 [128], P('kv'), may hold values from -3 to 1.5
- skip_scale: float32 [128], P('kv'), may hold values from 0.5 to 1.5
- output_gain: bfloat16 [8192], P('kv'), may hold values from 0.099609375 to 1.8984375
- output_weight: bfloat16 [8192, 4096], P('kv'), may hold values from -0.25 to 0.25
- saved_states: float32 [32, 5, 128, 64, 128], P('tp', None, 'kv'), may hold values from -1.8 to 1.8
- x_history: bfloat16 [32, 7, 8192], P('tp', None, 'kv'), may hold values from -6 to 6
- bc_history: bfloat16 [32, 7, 8192], P('tp', None, 'kv'), may hold values from -6 to 6
- accepted: int32 [32], P('tp'), may hold values from 0 to 4
Outputs:
- mixed: bfloat16 [128, 4096], P('tp', 'kv')
- new_states: float32 [32, 5, 128, 64, 128], P('tp', None, 'kv')
- x_window: bfloat16 [32, 7, 8192], P('tp', None, 'kv')
- bc_window: bfloat16 [32, 7, 8192], P('tp', None, 'kv')
All inputs are finite; a program needn't handle non-finite values.
Results may differ from a plain program's by a relative error of at most 0.02.
Values may be sent and summed in bfloat16 or wider, within the bound.
No kernel may reach another device: no remote copies, remote signals or barrier semaphores. Data moves between devices by JAX's collectives and lax.ppermute only.
A program may use at most 64 MiB of HBM per device.

v0:
```python
import jax
import jax.numpy as jnp
from jax import lax
from jax.sharding import Mesh
from jax.sharding import PartitionSpec as P

D = 4096
PROPS = 4
INNER = 8192
KV = ("kv_0", "kv_1", "kv_2")


EPSILON = 1e-05


def sent_to_all(value, axis):
    size = lax.axis_size(axis)
    return lax.all_to_all(
        jnp.broadcast_to(value[None], (size, *value.shape)), axis, 0, 0, tiled=True
    )


def over_copies(value, axis):
    return sent_to_all(value, axis).sum(axis=0)


def cut_along(value, dim, size):
    lengths = value.shape
    blocks = value.reshape(*lengths[:dim], size, lengths[dim] // size, *lengths[dim + 1 :])
    return jnp.moveaxis(blocks, dim, 0)


def sent_and_summed(value, axis, dim):
    blocks = cut_along(value, dim, lax.axis_size(axis))
    arrived = lax.all_to_all(blocks, axis, split_axis=0, concat_axis=0, tiled=True)
    return arrived.astype(jnp.float32).sum(axis=0)


def partner_2(block, axis, stride):
    count = lax.axis_size(axis)
    route = []
    for low in range(count):
        high = low | 1 << stride
        if high != low and high < count:
            route += [(low, high), (high, low)]
    return lax.ppermute(block, axis, route)


def one_axis_at_a_time(value, axes):
    far, near = axes
    nearer = over_copies(value, near)
    return over_copies(nearer, far)


def sent_and_summed_2(value, axis, dim):
    blocks = cut_along(value, dim, lax.axis_size(axis))
    arrived = lax.all_to_all(blocks, axis, split_axis=0, concat_axis=0, tiled=True)
    return arrived.sum(axis=0)


def summed_rows(value, axes, dim):
    far, near = axes
    own = sent_and_summed_2(cut_along(value, dim, lax.axis_size(far)), near, dim + 1)
    return jnp.sum(lax.all_to_all(own, far, 0, 0, tiled=True), axis=0)


def take_window(history, accepted, fresh_rows):
    history_len = history.shape[1] - fresh_rows.shape[1]
    indices = accepted[:, None] + jnp.arange(history_len, dtype=jnp.int32)[None, :]
    kept_rows = jnp.take_along_axis(history, indices[:, :, None], axis=1)
    return jnp.concatenate([kept_rows, fresh_rows], axis=1)


def conv_silu(window, kernel):
    length = window.shape[1] - kernel.shape[0] + 1
    running = window[:, 0:length].astype(jnp.float32) * kernel[0].astype(jnp.float32)
    for offset in range(1, kernel.shape[0]):
        running = running + window[:, offset : offset + length].astype(jnp.float32) * kernel[
            offset
        ].astype(jnp.float32)
    return jax.nn.silu(running)


def ssd_block(x_conv, step_size, decay_rate, b_terms, c_terms, first_state, skip_scale):
    cumulated = jnp.cumsum(-decay_rate * step_size, axis=1)
    length = x_conv.shape[1]
    indices = jnp.arange(length)
    causal = indices[:, None] >= indices[None, :]
    gaps = cumulated[:, :, None, :] - cumulated[:, None, :, :]
    weights = jnp.exp(jnp.where(causal[None, :, :, None], gaps, -jnp.inf))
    inputs = x_conv * step_size[..., None]
    outer_prod = jnp.einsum("srhp,srhn->srhpn", inputs, b_terms)
    states = jnp.exp(cumulated)[..., None, None] * first_state[:, None] + jnp.einsum(
        "strh,srhpn->sthpn", weights, outer_prod
    )
    output = jnp.einsum("sthn,sthpn->sthp", c_terms, states) + skip_scale[:, None] * x_conv
    return (output, states)


def local(
    hidden,
    input_gain,
    x_weight,
    z_weight,
    bc_weight,
    dt_weight,
    x_kernel,
    bc_kernel,
    dt_bias,
    decay_log,
    skip_scale,
    output_gain,
    output_weight,
    saved_states,
    x_history,
    bc_history,
    accepted,
):
    heads_here = dt_bias.shape[0]
    head_size = x_weight.shape[1] // heads_here
    state_size = saved_states.shape[4]
    seqs_here = accepted.shape[0]
    rows_here = hidden.shape[0] // lax.axis_size("tp")
    inner_here = x_weight.shape[1]
    bc_here = bc_weight.shape[1]
    widened = hidden.astype(jnp.float32)
    squares = over_copies(jnp.sum(widened * widened, axis=1), "tp")
    normed = (
        widened * lax.rsqrt(squares[:, None] / D + EPSILON) * input_gain.astype(jnp.float32)
    ).astype(jnp.bfloat16)
    weights = jnp.concatenate([x_weight, z_weight, bc_weight, dt_weight], axis=1)
    product = jnp.dot(normed, weights, preferred_element_type=jnp.float32)
    projected = sent_and_summed(
        lax.optimization_barrier(product.astype(jnp.bfloat16))
        .astype(jnp.float32)
        .astype(jnp.bfloat16),
        "tp",
        0,
    ).astype(jnp.bfloat16)
    x_fresh = projected[:, :inner_here]
    z_fresh = projected[:, inner_here : 2 * inner_here]
    bc_fresh = projected[:, 2 * inner_here : 2 * inner_here + bc_here]
    dt_fresh = projected[:, 2 * inner_here + bc_here :]
    x_window = take_window(x_history, accepted, x_fresh.reshape(seqs_here, PROPS, inner_here))
    bc_window = take_window(bc_history, accepted, bc_fresh.reshape(seqs_here, PROPS, bc_here))
    x_conv = conv_silu(x_window, x_kernel).reshape(seqs_here, PROPS, heads_here, head_size)
    bc_conv = conv_silu(bc_window, bc_kernel)
    spread = max(4 // heads_here, 1)
    position = lax.axis_index(KV)
    for level in range(spread.bit_length() - 1):
        partner = partner_2(bc_conv, KV, level)
        low_half = position // 2**level % 2 == 0
        bc_conv = jnp.where(
            low_half,
            jnp.concatenate([bc_conv, partner], axis=2),
            jnp.concatenate([partner, bc_conv], axis=2),
        )
    groups_here = bc_conv.shape[2] // (2 * state_size)
    paired = bc_conv.reshape(seqs_here, PROPS, groups_here, 2, state_size)
    per_group = heads_here // groups_here
    b_terms = jnp.repeat(paired[:, :, :, 0], per_group, axis=2)
    c_terms = jnp.repeat(paired[:, :, :, 1], per_group, axis=2)
    step_size = jax.nn.softplus(
        dt_fresh.astype(jnp.float32).reshape(seqs_here, PROPS, heads_here) + dt_bias
    )
    first_state = jnp.take_along_axis(saved_states, accepted[:, None, None, None, None], axis=1)[
        :, 0
    ]
    output, states = ssd_block(
        x_conv, step_size, jnp.exp(decay_log), b_terms, c_terms, first_state, skip_scale
    )
    new_states = jnp.concatenate([first_state[:, None], states], axis=1)
    gate_values = z_fresh.astype(jnp.float32).reshape(seqs_here, PROPS, heads_here, head_size)
    gated = (output * jax.nn.silu(gate_values)).reshape(rows_here, inner_here)
    square_sum = jnp.sum(gated * gated, axis=1)
    scaled = (gated * output_gain.astype(jnp.float32)).astype(jnp.bfloat16)
    partial_value = jnp.dot(scaled, output_weight, preferred_element_type=jnp.float32)
    total_squares = one_axis_at_a_time(square_sum, (("kv_0", "kv_1"), "kv_2"))
    summed = summed_rows(partial_value, (("kv_0", "kv_1"), "kv_2"), 1)
    mixed = (lax.rsqrt(total_squares / INNER + EPSILON)[:, None] * summed).astype(jnp.bfloat16)
    return (mixed, new_states, x_window, bc_window)


def solution(mesh):
    split = Mesh(mesh.devices.reshape(8, 8, 2, mesh.shape["tp"]), ("kv_0", "kv_1", "kv_2", "tp"))
    return jax.shard_map(
        local,
        mesh=split,
        in_specs=(
            P(None, "tp"),
            P("tp"),
            P("tp", KV),
            P("tp", KV),
            P("tp", KV),
            P("tp", KV),
            P(None, KV),
            P(None, KV),
            P(KV),
            P(KV),
            P(KV),
            P(KV),
            P(KV, None),
            P("tp", None, KV, None, None),
            P("tp", None, KV),
            P("tp", None, KV),
            P("tp"),
        ),
        out_specs=(
            P("tp", KV),
            P("tp", None, KV, None, None),
            P("tp", None, KV),
            P("tp", None, KV),
        ),
        check_vma=False,
    )
```

profile of v0, /device:TPU:1, one launch (start us, length us, event | category | flops | bytes accessed | tf_op | source)
XLA Modules:
  0.0 101.7 jit_solution(16168655335332894303)
XLA Ops:
  0.7 1.2 %fusion.4 = f32[128]{0:T(128)S(1)} fusion(bf16[128,1024]{1,0:T(8,128)(2,1)} %param.19), kind=kLoop, calls=%fused_computation.13 | loop fusion | flops 393088 | bytes 262656 | tf_op jit(solution)/shard_map/reduce_sum | solution.py:127
  1.9 0.6 broadcast_in_dim.34
  2.5 4.8 %all-to-all-start = ((f32[4,1,128]{2,1,0:T(1,128)}), f32[4,1,128]{2,1,0:T(1,128)S(1)}, u32[]{:S(2)}, u32[]{:S(2)}) async-start(f32[4,1,128]{2,1,0:T(1,128)} %broadcast_in_dim.34), calls=%async_computation | async-start | bytes 4096 | tf_op jit(solution)/shard_map/all_to_all | solution.py:18
  7.3 0.7 compare_and_fusion
  8.0 0.7 fusion.39
  8.6 0.7 fusion.42
  9.3 0.7 shift-left_or_fusion
  10.2 0.8 bitcast_convert_fusion.3
  11.1 1.5 %gather_fusion.2 = bf16[24,64]{1,0:T(8,128)(2,1)S(1)} fusion(bf16[8,7,64]{2,0,1:T(8,128)(2,1)} %param.33, s32[24]{0:T(128)S(1)} %reshape.409), kind=kCustom, calls=%fused_computation.1.clone | custom fusion | bytes 6336 | tf_op jit(solution)/shard_map/jit(take_along_axis)/gather | solution.py:70
  12.6 1.5 %gather_fusion.1 = bf16[24,64]{1,0:T(8,128)(2,1)S(1)} fusion(bf16[8,7,64]{2,0,1:T(8,128)(2,1)} %param.34, s32[24]{0:T(128)S(1)} %reshape.409), kind=kCustom, calls=%fused_computation.clone | custom fusion | bytes 6336 | tf_op jit(solution)/shard_map/jit(take_along_axis)/gather | solution.py:70
  14.1 0.6 gather_fusion
  14.9 0.8 bitcast_convert_fusion.7
  15.7 0.7 convert_element_type.138
  16.4 1.5 %convolution_convert_fusion = bf16[128,193]{0,1:T(8,128)(2,1)S(1)} fusion(bf16[1024,1]{0,1:T(2,128)(2,1)} %param.24, bf16[1024,64]{0,1:T(8,128)(2,1)} %param.23, bf16[1024,64]{0,1:T(8,128)(2,1)} %param.22, bf16[1024,64]{0,1:T(8,128)(2,1)} %param.21, bf16[128,1024]{1,0:T(8,128)(2,1)} %param.19, f32[1024]{0:T(1024)S(1)} %convert_element_type.138, ...), kind=kOutput, calls=%fused_computation.7 | convolution fusion | flops 52723840 | bytes 711424 | tf_op jit(solution)/shard_map/dot_general | solution.py:132
  17.9 0.7 copy.102
  18.7 4.2 %all-to-all-start.1 = ((bf16[4,32,193]{2,1,0:T(8,128)(2,1)}), bf16[4,32,193]{2,1,0:T(8,128)(2,1)S(1)}, u32[]{:S(2)}, u32[]{:S(2)}) async-start(bf16[4,32,193]{2,1,0:T(8,128)(2,1)} %bitcast.2), calls=%async_computation.1 | async-start | bytes 131072 | tf_op jit(solution)/shard_map/all_to_all | solution.py:35
  24.9 0.5 copy.120
  25.4 2.0 %all-to-all-done.1 = bf16[4,32,193]{2,1,0:T(8,128)(2,1)S(1)} async-done(((bf16[4,32,193]{2,1,0:T(8,128)(2,1)}), bf16[4,32,193]{2,1,0:T(8,128)(2,1)S(1)}, u32[]{:S(2)}, u32[]{:S(2)}) %all-to-all-start.1) | async-done | bytes 49440 | tf_op jit(solution)/shard_map/all_to_all | solution.py:35
  27.8 8.8 %collective-permute-start = (f32[8,4,64]{2,1,0:T(4,128)S(1)}, f32[8,4,64]{2,1,0:T(4,128)S(1)}, u32[]{:S(2)}, u32[]{:S(2)}) collective-permute-start(f32[8,4,64]{2,1,0:T(4,128)S(1)} %divide_multiply_fusion.1), channel_id=1, source_target_pairs={{0,4},{4,0},{8,12},{12,8},{16,20},{20,16},{24,28},{28,24},{32,36},... | collective-permute-start | bytes 24584 | tf_op jit(solution)/shard_map/ppermute | solution.py:46
  36.7 0.8 collective-permute-done
  37.5 1.9 %collective-permute-start.1 = (f32[8,4,128]{2,1,0:T(4,128)S(1)}, f32[8,4,128]{2,1,0:T(4,128)S(1)}, u32[]{:S(2)}, u32[]{:S(2)}) collective-permute-start(f32[8,4,128]{2,1,0:T(4,128)S(1)} %maximum_select_fusion.1), channel_id=1, source_target_pairs={{0,8},{8,0},{4,12},{12,4},{16,24},{24,16},{20,28},{28,20},{32,40},... | collective-permute-start | bytes 49160 | tf_op jit(solution)/shard_map/ppermute | solution.py:46
  39.9 2.2 %collective-permute-done.1 = f32[8,4,128]{2,1,0:T(4,128)S(1)} collective-permute-done((f32[8,4,128]{2,1,0:T(4,128)S(1)}, f32[8,4,128]{2,1,0:T(4,128)S(1)}, u32[]{:S(2)}, u32[]{:S(2)}) %collective-permute-start.1) | collective-permute-done | bytes 16416 | tf_op jit(solution)/shard_map/ppermute | solution.py:46
  42.1 1.0 fusion
  43.1 1.0 copy-done.3
  44.0 0.4 fusion.1
  44.6 4.8 %all_to_all.33 = f32[2,1,32]{2,1,0:T(1,128)S(1)} all-to-all(f32[2,1,32]{2,1,0:T(1,128)S(1)} %broadcast_in_dim.44), channel_id=1, replica_groups=mesh['kv_0'=8,'kv_1'=8,'kv_2'=2,'tp'=4] {'kv_2'}, dimensions={0} | all-to-all | bytes 512 | tf_op jit(solution)/shard_map/all_to_all | solution.py:18
  49.5 1.1 %convolution_bitcast_fusion = f32[64,32,64]{2,1,0:T(8,128)S(1)} fusion(bf16[32,64,1]{1,0,2:T(8,128)(2,1)S(1)} %bitcast.99, bf16[64,64,64]{2,1,0:T(8,128)(2,1)S(1)} %bitcast.89), kind=kOutput, calls=%fused_computation.4 | convolution fusion | flops 16777216 | bytes 1052672 | tf_op jit(solution)/shard_map/dot_general | solution.py:177
  50.6 0.6 copy.109
  51.3 0.7 reshape.422
  52.0 4.1 %all_to_all.34 = f32[2,1,65536]{2,1,0:T(1,128)S(1)} all-to-all(f32[2,1,65536]{2,1,0:T(1,128)S(1)} %reshape.422), channel_id=1, replica_groups=mesh['kv_0'=8,'kv_1'=8,'kv_2'=2,'tp'=4] {'kv_2'}, dimensions={0} | all-to-all | bytes 1048576 | tf_op jit(solution)/shard_map/all_to_all | solution.py:57
  56.1 0.6 broadcast_in_dim.45
  56.7 12.1 %all-to-all-start.3 = ((f32[64,1,32]{2,1,0:T(1,128)}), f32[64,1,32]{2,1,0:T(1,128)S(1)}, u32[]{:S(2)}, u32[]{:S(2)}) async-start(f32[64,1,32]{2,1,0:T(1,128)} %broadcast_in_dim.45), calls=%async_computation.3 | async-start | bytes 65536 | tf_op jit(solution)/shard_map/all_to_all | solution.py:18
  68.8 0.5 broadcast.283
  69.3 2.3 %reduce.9 = f32[2,65536]{1,0:T(2,128)S(1)} reduce(f32[2,1,65536]{2,1,0:T(1,128)S(1)} %all_to_all.34, f32[]{:T(128)} %broadcast.283), dimensions={1}, to_apply=%all_to_all.25.reduce_sub_computation | reduce | bytes 1048580 | tf_op jit(solution)/shard_map/all_to_all | solution.py:57
  71.6 0.6 reshape.423
  72.4 0.9 copy.112
  73.3 1.2 %reshape.424 = f32[64,1,1024]{2,1,0:T(1,128)} reshape(f32[64,32,32]{2,1,0:T(8,128)S(1)} %copy.112) | data formatting | bytes 524288
  74.5 5.2 %all-to-all-done.3 = f32[64,1,32]{2,1,0:T(1,128)S(1)} async-done(((f32[64,1,32]{2,1,0:T(1,128)}), f32[64,1,32]{2,1,0:T(1,128)S(1)}, u32[]{:S(2)}, u32[]{:S(2)}) %all-to-all-start.3) | async-done | bytes 8224 | tf_op jit(solution)/shard_map/all_to_all | solution.py:18
  79.6 7.0 %all-to-all-start.5 = ((f32[64,1,1024]{2,1,0:T(1,128)}), f32[64,1,1024]{2,1,0:T(1,128)S(1)}, u32[]{:S(2)}, u32[]{:S(2)}) async-start(f32[64,1,1024]{2,1,0:T(1,128)} %reshape.424), calls=%async_computation.5 | async-start | bytes 524288 | tf_op jit(solution)/shard_map/all_to_all | solution.py:64
  86.6 0.3 broadcast_select_fusion
  86.9 0.6 copy.115
  87.6 0.6 copy.114
  88.2 1.7 %pad_maximum_fusion = f32[8,5,1,64,128]{4,1,3,0,2:T(8,128)S(1)} fusion(f32[8,4,1,64,128]{4,1,3,0,2:T(4,128)} %copy-done.3, f32[8,1,1,64,128]{4,1,3,0,2:T(1,128)S(1)} %broadcast_select_fusion), kind=kLoop, calls=%fused_computation.3 | loop fusion | flops 327680 | bytes 2621440 | tf_op jit(solution)/shard_map/concatenate | solution.py:172
  89.8 1.3 %copy.113 = f32[8,5,1,64,128]{4,3,2,1,0:T(8,128)} copy(f32[8,5,1,64,128]{4,1,3,0,2:T(8,128)S(1)} %pad_maximum_fusion) | data formatting | bytes 2621440
  91.2 8.1 %all-to-all-done.5 = f32[64,1,1024]{2,1,0:T(1,128)S(1)} async-done(((f32[64,1,1024]{2,1,0:T(1,128)}), f32[64,1,1024]{2,1,0:T(1,128)S(1)}, u32[]{:S(2)}, u32[]{:S(2)}) %all-to-all-start.5) | async-done | bytes 262176 | tf_op jit(solution)/shard_map/all_to_all | solution.py:64
  99.3 1.3 %reduce.10 = f32[64,1024]{1,0:T(8,128)S(1)} reduce(f32[64,1,1024]{2,1,0:T(1,128)S(1)} %all-to-all-done.5, f32[]{:T(128)} %broadcast.283), dimensions={1}, to_apply=%all_to_all.26.reduce_sub_computation | reduce | bytes 524292 | tf_op jit(solution)/shard_map/all_to_all | solution.py:64
  100.5 0.3 reshape.425
  101.0 0.7 multiply_convert_fusion
  (51 shorter events, 2.2 us)
Async XLA Ops:
  0.6 13.5 %copy-start = (f32[8,5,1,64,128]{4,3,2,1,0:T(8,128)S(1)}, f32[8,5,1,64,128]{4,3,2,1,0:T(8,128)}, u32[]{:S(2)}) copy-start(f32[8,5,1,64,128]{4,3,2,1,0:T(8,128)} %param.32) | copy-start | bytes 3932164
  0.6 24.3 %copy-start.5 = (bf16[64]{0:T(256)(128)(2,1)S(1)}, bf16[64]{0:T(256)(128)(2,1)}, u32[]{:S(2)}) copy-start(bf16[64]{0:T(256)(128)(2,1)} %param.30) | copy-start | bytes 388
  0.7 24.3 %copy-start.4 = (bf16[64,4096]{1,0:T(8,128)(2,1)S(1)}, bf16[64,4096]{1,0:T(8,128)(2,1)}, u32[]{:S(2)}) copy-start(bf16[64,4096]{1,0:T(8,128)(2,1)} %param.31) | copy-start | bytes 1572868
  2.5 13.9 %all-to-all-start = ((f32[4,1,128]{2,1,0:T(1,128)}), f32[4,1,128]{2,1,0:T(1,128)S(1)}, u32[]{:S(2)}, u32[]{:S(2)}) async-start(f32[4,1,128]{2,1,0:T(1,128)} %broadcast_in_dim.34), calls=%async_computation | async-start | bytes 4096 | tf_op jit(solution)/shard_map/all_to_all | solution.py:18
  14.7 10.2 %copy-start.1 = (f32[8,64,128]{2,1,0:T(8,128)}, f32[8,64,128]{2,1,0:T(8,128)S(1)}, u32[]{:S(2)}) copy-start(f32[8,64,128]{2,1,0:T(8,128)S(1)} %gather_fusion) | copy-start | bytes 786436
  18.7 8.7 %all-to-all-start.1 = ((bf16[4,32,193]{2,1,0:T(8,128)(2,1)}), bf16[4,32,193]{2,1,0:T(8,128)(2,1)S(1)}, u32[]{:S(2)}, u32[]{:S(2)}) async-start(bf16[4,32,193]{2,1,0:T(8,128)(2,1)} %bitcast.2), calls=%async_computation.1 | async-start | bytes 131072 | tf_op jit(solution)/shard_map/all_to_all | solution.py:35
  27.8 9.6 %collective-permute-start = (f32[8,4,64]{2,1,0:T(4,128)S(1)}, f32[8,4,64]{2,1,0:T(4,128)S(1)}, u32[]{:S(2)}, u32[]{:S(2)}) collective-permute-start(f32[8,4,64]{2,1,0:T(4,128)S(1)} %divide_multiply_fusion.1), channel_id=1, source_target_pairs={{0,4},{4,0},{8,12},{12,8},{16,20},{20,16},{24,28},{28,24},{32,36},... | collective-permute-start | bytes 24584 | tf_op jit(solution)/shard_map/ppermute | solution.py:46
  37.5 4.5 %collective-permute-start.1 = (f32[8,4,128]{2,1,0:T(4,128)S(1)}, f32[8,4,128]{2,1,0:T(4,128)S(1)}, u32[]{:S(2)}, u32[]{:S(2)}) collective-permute-start(f32[8,4,128]{2,1,0:T(4,128)S(1)} %maximum_select_fusion.1), channel_id=1, source_target_pairs={{0,8},{8,0},{4,12},{12,4},{16,24},{24,16},{20,28},{28,20},{32,40},... | collective-permute-start | bytes 49160 | tf_op jit(solution)/shard_map/ppermute | solution.py:46
  43.1 1.0 copy-start.3
  56.7 22.9 %all-to-all-start.3 = ((f32[64,1,32]{2,1,0:T(1,128)}), f32[64,1,32]{2,1,0:T(1,128)S(1)}, u32[]{:S(2)}, u32[]{:S(2)}) async-start(f32[64,1,32]{2,1,0:T(1,128)} %broadcast_in_dim.45), calls=%async_computation.3 | async-start | bytes 65536 | tf_op jit(solution)/shard_map/all_to_all | solution.py:18
  72.4 14.3 %copy-start.2 = (f32[8,64,128]{2,1,0:T(8,128)S(1)}, f32[8,64,128]{2,1,0:T(8,128)}, u32[]{:S(2)}) copy-start(f32[8,64,128]{2,1,0:T(8,128)} %copy-done.1) | copy-start | bytes 786436
  79.6 19.6 %all-to-all-start.5 = ((f32[64,1,1024]{2,1,0:T(1,128)}), f32[64,1,1024]{2,1,0:T(1,128)S(1)}, u32[]{:S(2)}, u32[]{:S(2)}) async-start(f32[64,1,1024]{2,1,0:T(1,128)} %reshape.424), calls=%async_computation.5 | async-start | bytes 524288 | tf_op jit(solution)/shard_map/all_to_all | solution.py:64
where the time goes:
time: 104 us; the launch traced here: 102 us
  starting transfers between devices  38.8 us (37%)
  waiting for transfers between devices  18.1 us (17%)
  local copies, waits for them, and re-layouts  15.2 us (15%)
  other arithmetic  13.7 us (13%)
  blocking collectives  8.97 us (9%)
  matrix products  3.9 us (4%)
  between operations  2.93 us (3%)
    all_to_all x2, starting transfers between devices, sent_to_all(): lax.all_to_all(jnp.broadcast_to(value[None], (size, *value.shape)), axis,...  16.9 us
    ppermute x2, starting transfers between devices, partner_2(): return lax.ppermute(block, axis, route)  10.7 us
    all_to_all x1, waiting for transfers between devices, summed_rows(): return jnp.sum(lax.all_to_all(own, far, 0, 0, tiled=True), axis=0)  8.07 us
    all_to_all x1, starting transfers between devices, summed_rows(): return jnp.sum(lax.all_to_all(own, far, 0, 0, tiled=True), axis=0)  6.97 us
    unnamed x20, local copies, waits for them, and re-layouts  6.3 us
    all_to_all x2, waiting for transfers between devices, sent_to_all(): lax.all_to_all(jnp.broadcast_to(value[None], (size, *value.shape)), axis,...  5.17 us
    all_to_all x1, blocking collectives, sent_to_all(): lax.all_to_all(jnp.broadcast_to(value[None], (size, *value.shape)), axis,...  4.85 us
    all_to_all x1, starting transfers between devices, sent_and_summed(): lax.all_to_all(blocks, axis, split_axis=0, concat_axis=0, tiled=True)  4.24 us
  transfers between devices with their start and end apart: 6, of which 5 were waited for; matrix products, arithmetic and copies ran while one was open for 20% of the time, Pallas kernels for 0%

commit v1 on v0

v1 whole, which is shorter than its diff:
```python
import jax
import jax.numpy as jnp
from jax import lax
from jax.experimental import pallas as pl
from jax.experimental.pallas import tpu as pltpu
from jax.sharding import Mesh
from jax.sharding import PartitionSpec as P

D = 4096
PROPS = 4
INNER = 8192
KV = ("z", "yh", "yl", "c")
NEAR = ("yl", "c", "tp")
EPSILON = 1e-05
TP = 4
NEAR_KV = 4
KV_SIZE = 128
SEQS = 8
TOKENS = 32
HEAD = 64
STATE = 128
LINES = 10

F32 = jnp.float32
BF16 = jnp.bfloat16


def rounded(value):
    return value.astype(BF16).astype(F32)


def lanes_of(shape):
    return lax.broadcasted_iota(jnp.int32, shape, len(shape) - 1)


def rows_of(shape):
    return lax.broadcasted_iota(jnp.int32, shape, len(shape) - 2)


def dot_nt(a, b):
    return lax.dot_general(a, b, (((1,), (1,)), ((), ())), preferred_element_type=F32)


def silu(v):
    return v / (1.0 + jnp.exp(-v))


def accepted_column(accepted, shape):
    rows = rows_of(shape)
    column = jnp.zeros(shape, jnp.int32)
    for s in range(SEQS):
        column = jnp.where(rows == s, accepted[s], column)
    return column


def kept_rows(history, column):
    whole = [history[i].astype(F32) for i in range(7)]
    kept = []
    for m in range(3):
        row = whole[m]
        for a in range(1, PROPS + 1):
            row = jnp.where(column == a, whole[m + a], row)
        kept.append(row)
    return kept


def project_body(
    accepted, hidden, gain, x_weight, z_weight, bc_weight, dt_weight, bc_history, bc_kernel, message, first, second
):
    widened = hidden[...].astype(F32)
    scaled = (widened * gain[...].astype(F32)[None, :]).astype(BF16)
    squares = jnp.sum(widened * widened, axis=1, keepdims=True)
    dt_rows = jnp.broadcast_to(dt_weight[...], (HEAD, dt_weight.shape[1]))
    first[...] = dot_nt(scaled, jnp.concatenate([x_weight[...], z_weight[...]], axis=0))
    last = dot_nt(scaled, jnp.concatenate([bc_weight[...], dt_rows], axis=0))
    second[...] = last
    turned = jnp.transpose(jnp.where(lanes_of((128, 128)) == HEAD + 1, squares, last))
    dt_line = jnp.broadcast_to(turned[HEAD : HEAD + 1], (8, 128))
    square_line = jnp.broadcast_to(turned[HEAD + 1 : HEAD + 2], (8, 128))
    square_high = rounded(square_line)
    rows = rows_of((8, 128))
    upper = lanes_of((8, 128)) >= HEAD
    lines = jnp.where(rows == 4, dt_line, jnp.where(rows == 5, square_high, square_line - square_high))
    column = accepted_column(accepted, (SEQS, HEAD))
    empty = jnp.zeros((SEQS, HEAD), F32)
    extra = [jnp.concatenate([empty, row], axis=1) for row in kept_rows(bc_history, column)]
    taps = jnp.concatenate([bc_kernel[...].astype(F32), jnp.zeros((4, HEAD), F32)], axis=0)
    taps = jnp.concatenate([empty, taps], axis=1)
    for j in range(TP):
        top = [first[pl.ds(TOKENS * j + t, SEQS, stride=PROPS), :] for t in range(PROPS)]
        low = [second[pl.ds(TOKENS * j + t, SEQS, stride=PROPS), :] for t in range(PROPS)]
        ending = jnp.where(rows < 4, taps, pltpu.roll(lines, (64 - 32 * j) % 128, 1))
        low = [jnp.where(upper, e, v) for e, v in zip([*extra, ending], low)]
        block = jnp.concatenate(top + low, axis=0).astype(BF16)
        for g in range(NEAR_KV):
            message[g * TP + j] = block


def prepare_body(accepted, saved, weight, first_state, turned_weight, arrivals):
    copies = [
        pltpu.make_async_copy(saved.at[s, accepted[s], 0], first_state.at[s], arrivals.at[s]) for s in range(SEQS)
    ]
    for copy in copies:
        copy.start()
    gap = jnp.zeros((LINES - 8, 256), F32)

    def turn(i, _):
        block = weight[:, pl.ds(pl.multiple_of(i * 256, 256), 256)].astype(F32)
        turned = jnp.transpose(block)
        pieces = []
        for d in range(8):
            quarter = [turned[32 * d + 8 * q : 32 * d + 8 * q + 8] for q in range(4)]
            pieces += [jnp.concatenate(quarter, axis=1), gap]
        turned_weight[pl.ds(pl.multiple_of(i * 8 * LINES, 16), 8 * LINES), :] = jnp.concatenate(pieces, axis=0).astype(
            BF16
        )
        return 0

    lax.fori_loop(0, weight.shape[1] // 256, turn, 0)
    for copy in copies:
        copy.wait()


def mix_body(
    accepted,
    dt_bias,
    decay_log,
    skip_scale,
    arrived,
    first_state,
    turned_weight,
    x_kernel,
    x_history,
    output_gain,
    message,
    x_window,
    bc_window,
    inputs_out,
    b_out,
    decay_out,
    columns,
    ordered,
    square_rows,
):
    place = lax.axis_index(("yl", "c"))
    mine = lax.axis_index("tp")
    tile = (SEQS, 128)
    lanes = lanes_of(tile)
    rows = rows_of(tile)
    lower = lanes < HEAD

    def tiles(value):
        return [value[8 * i : 8 * i + 8] for i in range(value.shape[0] // 8)]

    own = arrived[place * TP].astype(F32)
    for k in range(1, TP):
        own = own + arrived[place * TP + k].astype(F32)
    own = tiles(own)
    ending = own[7]
    mean = (ending[5:6] + ending[6:7]) / D
    lined = jnp.where(rows == 5, jnp.broadcast_to(lax.rsqrt(mean + EPSILON), tile), ending)
    columns[...] = jnp.transpose(lined)[HEAD : HEAD + TOKENS]
    scale, step, cumulated = [], [], []
    rate = jnp.exp(jnp.full((SEQS, 1), decay_log[0], F32))
    total = jnp.zeros((SEQS, 1), F32)
    for t in range(PROPS):
        column = columns[pl.ds(t, SEQS, stride=PROPS), :]
        scale.append(column[:, 5:6])
        raw = rounded(column[:, 5:6] * column[:, 4:5]) + dt_bias[0]
        step.append(jnp.maximum(raw, 0.0) + jnp.log1p(jnp.exp(-jnp.abs(raw))))
        total = total - rate * step[t]
        cumulated.append(total)
    fresh = [rounded(scale[t] * own[t]) for t in range(PROPS)]
    sums, extras = [], []
    for g in range(NEAR_KV):
        group = arrived[g * TP, 32:64, :].astype(F32)
        for k in range(1, TP):
            group = group + arrived[g * TP + k, 32:64, :].astype(F32)
        sums.append(tiles(group))
        extras.append(tiles(arrived[g * TP + mine, 32:64, :].astype(F32)))

    def convolved(window, taps):
        results = []
        for t in range(PROPS):
            running = window[t] * taps[0:1]
            for j in range(1, 4):
                running = running + window[t + j] * taps[j : j + 1]
            results.append(silu(running))
        return results

    def terms(left, right):
        window = [
            jnp.where(lower, pltpu.roll(extras[left][m], HEAD, 1), extras[right][m]) for m in range(4)
        ]
        new = [
            rounded(scale[t] * jnp.where(lower, sums[left][t], pltpu.roll(sums[right][t], HEAD, 1)))
            for t in range(PROPS)
        ]
        return convolved(window[:3] + new, window[3])

    b_terms = terms(0, 1)
    c_terms = terms(2, 3)
    column = accepted_column(accepted, (SEQS, HEAD))
    kept = kept_rows(x_history, column)
    empty = jnp.zeros((SEQS, HEAD), F32)
    x_taps = jnp.concatenate([x_kernel[...].astype(F32), jnp.zeros((4, HEAD), F32)], axis=1)
    x_conv = convolved([jnp.concatenate([row, empty], axis=1) for row in kept] + fresh, x_taps)
    states = first_state[...].reshape(SEQS * HEAD, STATE).astype(BF16)
    read = dot_nt(jnp.concatenate(c_terms, axis=0).astype(BF16), states)
    gain = output_gain[...].astype(F32)
    for t in range(PROPS):
        picked = jnp.zeros(tile, F32)
        for k in range(SEQS // 2):
            picked = jnp.where(rows // 2 == k, read[8 * t : 8 * t + 8, 128 * k : 128 * k + 128], picked)
        picked = jnp.where(rows % 2 == 0, picked, pltpu.roll(picked, HEAD, 1))
        output = jnp.exp(cumulated[t]) * picked
        for r in range(t + 1):
            product = jnp.sum(c_terms[t] * b_terms[r], axis=1, keepdims=True)
            output = output + (jnp.exp(cumulated[t] - cumulated[r]) * step[r] * product) * x_conv[r]
        output = output + skip_scale[0] * x_conv[t]
        gated = jnp.where(lower, output * silu(pltpu.roll(fresh[t], HEAD, 1)), 0.0)
        square = jnp.sum(gated * gated, axis=1, keepdims=True)
        ordered[pl.ds(t, SEQS, stride=PROPS), :] = gated
        square_rows[pl.ds(t, SEQS, stride=PROPS), :] = jnp.broadcast_to(square, tile)
        inputs_out[8 * t : 8 * t + 8, :] = x_conv[t] * step[t]
        b_out[8 * t : 8 * t + 8, :] = b_terms[t]
        decay_out[8 * t : 8 * t + 8, :] = jnp.broadcast_to(jnp.exp(-rate * step[t]), tile)
    scaled = ordered[...] * jnp.concatenate([gain, gain], axis=1)
    scaled = scaled.astype(BF16)
    moved = pltpu.roll(ordered[...], HEAD, 1) * jnp.concatenate([gain, gain], axis=1)
    moved = moved.astype(BF16)
    none = jnp.zeros((TOKENS, 128), BF16)
    spread = jnp.concatenate(
        [
            jnp.concatenate([scaled, none], axis=1),
            jnp.concatenate([moved, none], axis=1),
            jnp.concatenate([none, scaled], axis=1),
            jnp.concatenate([none, moved], axis=1),
        ],
        axis=0,
    )
    squares = square_rows[...]
    square_line = jnp.transpose(jnp.concatenate([squares] * 4, axis=0))[0:1]
    high = rounded(square_line)
    low = square_line - high
    period = 4 * LINES
    spot = rows_of((period, 128)) % LINES
    lines = jnp.where(spot == 8, high, jnp.where(spot == 9, low, 0.0))
    part = 8 * period
    lines = jnp.concatenate([lines] * 8, axis=0)
    for i in range(turned_weight.shape[0] // part):
        product = dot_nt(turned_weight[part * i : part * (i + 1), :], spread)
        message[part * i : part * (i + 1), :] = (product + lines).astype(BF16)
    own_extra = tiles(arrived[place * TP + mine, 32:64, :].astype(F32))
    for m in range(3):
        x_window[m] = kept[m].astype(BF16)
        bc_window[m] = pltpu.roll(own_extra[m], HEAD, 1)[:, :HEAD].astype(BF16)
    for t in range(PROPS):
        x_window[3 + t] = fresh[t][:, :HEAD].astype(BF16)
        bc_window[3 + t] = (scale[t] * own[4 + t])[:, :HEAD].astype(BF16)


def state_body(inputs, b_terms, decay, first_state, new_states):
    padded = jnp.concatenate([inputs[...], jnp.zeros((128 - TOKENS, 128), F32)], axis=0)
    turned = jnp.transpose(padded)[:HEAD]
    for s in range(SEQS):
        state = first_state[s]
        new_states[s, 0, 0] = state
        for t in range(PROPS):
            at = 8 * t + s
            state = state * decay[at : at + 1, :] + turned[:, at : at + 1] * b_terms[at : at + 1, :]
            new_states[s, t + 1, 0] = state


def finish_body(arrived, mixed, total):
    step = 8 * LINES
    running = arrived[0:step, :].astype(F32)
    for i in range(1, arrived.shape[0] // step):
        running = running + arrived[step * i : step * (i + 1), :].astype(F32)
    total[...] = running
    summed = total[0:8, :]
    squares = total[8:10, :]
    for i in range(1, 8):
        summed = summed + total[LINES * i : LINES * i + 8, :]
        squares = squares + total[LINES * i + 8 : LINES * i + 10, :]
    mean = (squares[0:1] + squares[1:2]) / INNER
    summed = summed * lax.rsqrt(mean + EPSILON)
    stacked = jnp.concatenate([summed] + [pltpu.roll(summed, 128 - 32 * q, 1) for q in range(1, 4)], axis=0)
    mixed[...] = jnp.transpose(stacked)[:TOKENS].astype(BF16)


def smem():
    return pl.BlockSpec(memory_space=pltpu.SMEM)


def vmem():
    return pl.BlockSpec(memory_space=pltpu.VMEM)


def local(
    hidden,
    input_gain,
    x_weight,
    z_weight,
    bc_weight,
    dt_weight,
    x_kernel,
    bc_kernel,
    dt_bias,
    decay_log,
    skip_scale,
    output_gain,
    output_weight,
    saved_states,
    x_history,
    bc_history,
    accepted,
):
    shape = jax.ShapeDtypeStruct
    lines = KV_SIZE * LINES
    x_rows = jnp.transpose(x_history, (1, 0, 2))
    bc_rows = jnp.transpose(bc_history, (1, 0, 2))
    with jax.named_scope("project"):
        near = pl.pallas_call(
            project_body,
            out_shape=shape((TP * NEAR_KV, 2 * TOKENS, 128), BF16),
            in_specs=[smem()] + [vmem()] * 8,
            out_specs=vmem(),
            scratch_shapes=[pltpu.VMEM((128, 128), F32), pltpu.VMEM((128, 128), F32)],
        )(accepted, hidden, input_gain, x_weight.T, z_weight.T, bc_weight.T, dt_weight.T, bc_rows, bc_kernel)
    with jax.named_scope("near"):
        arrived = lax.all_to_all(near, NEAR, 0, 0, tiled=True)
    with jax.named_scope("prepare"):
        first_state, turned_weight = pl.pallas_call(
            prepare_body,
            out_shape=(shape((SEQS, HEAD, STATE), F32), shape((lines, 256), BF16)),
            in_specs=[smem(), pl.BlockSpec(memory_space=pl.ANY), vmem()],
            out_specs=(vmem(), vmem()),
            scratch_shapes=[pltpu.SemaphoreType.DMA((SEQS,))],
            cost_estimate=pl.CostEstimate(flops=4_000_000, bytes_accessed=3_000_000, transcendentals=0),
        )(accepted, saved_states, output_weight)
        gain_row = output_gain.reshape(1, HEAD)
    with jax.named_scope("mix"):
        far, x_window, bc_window, inputs, b_terms, decay = pl.pallas_call(
            mix_body,
            out_shape=(
                shape((lines, 128), BF16),
                shape((7, SEQS, HEAD), BF16),
                shape((7, SEQS, HEAD), BF16),
                shape((TOKENS, 128), F32),
                shape((TOKENS, 128), F32),
                shape((TOKENS, 128), F32),
            ),
            in_specs=[smem()] * 4 + [vmem()] * 6,
            out_specs=(vmem(),) * 6,
            scratch_shapes=[
                pltpu.VMEM((TOKENS, 8), F32),
                pltpu.VMEM((TOKENS, 128), F32),
                pltpu.VMEM((TOKENS, 128), F32),
            ],
        )(
            accepted,
            dt_bias,
            decay_log,
            skip_scale,
            arrived,
            first_state,
            turned_weight,
            x_kernel,
            x_rows,
            gain_row,
        )
    with jax.named_scope("far"):
        landed = lax.all_to_all(far.reshape(KV_SIZE, LINES // 2, 2, 128), KV, 0, 0, tiled=True)
    with jax.named_scope("states"):
        new_states = pl.pallas_call(
            state_body,
            out_shape=shape((SEQS, PROPS + 1, 1, HEAD, STATE), F32),
            in_specs=[vmem()] * 4,
            out_specs=vmem(),
            cost_estimate=pl.CostEstimate(flops=4_000_000, bytes_accessed=3_000_000, transcendentals=0),
        )(inputs, b_terms, decay, first_state)
    with jax.named_scope("finish"):
        mixed = pl.pallas_call(
            finish_body,
            out_shape=shape((TOKENS, TOKENS), BF16),
            in_specs=[vmem()],
            out_specs=vmem(),
            scratch_shapes=[pltpu.VMEM((8 * LINES, 128), F32)],
        )(landed.reshape(lines, 128))
    return (mixed, new_states, jnp.transpose(x_window, (1, 0, 2)), jnp.transpose(bc_window, (1, 0, 2)))


def solution(mesh):
    split = Mesh(mesh.devices.reshape(8, 4, 2, 2, mesh.shape["tp"]), ("z", "yh", "yl", "c", "tp"))
    return jax.shard_map(
        local,
        mesh=split,
        in_specs=(
            P(None, "tp"),
            P("tp"),
            P("tp", KV),
            P("tp", KV),
            P("tp", KV),
            P("tp", KV),
            P(None, KV),
            P(None, KV),
            P(KV),
            P(KV),
            P(KV),
            P(KV),
            P(KV, None),
            P("tp", None, KV, None, None),
            P("tp", None, KV),
            P("tp", None, KV),
            P("tp"),
        ),
        out_specs=(
            P("tp", KV),
            P("tp", None, KV, None, None),
            P("tp", None, KV),
            P("tp", None, KV),
        ),
        check_vma=False,
    )
```

time: 104 us -> 56.6 us (0.54); the launches traced: 102 us -> 56.2 us
  starting transfers between devices: 38.8 us -> 23.2 us
  Pallas kernels: 0 us -> 14.4 us
  local copies, waits for them, and re-layouts: 15.2 us -> 1.43 us
  other arithmetic: 13.7 us -> 0 us
  blocking collectives: 8.97 us -> 0 us
  matrix products: 3.9 us -> 0 us
  waiting for transfers between devices: 18.1 us -> 14.6 us
    pallas_call x0 -> x5, Pallas kernels: none -> 14.4 us  [the longest x1 4.94 us: local(): pl.pallas_call(prepare_body, out_shape=(shape((SEQS, HEAD, STATE), F32),...]
    ppermute x2 -> x0, starting transfers between devices: 10.7 us -> none  [partner_2(): return lax.ppermute(block, axis, route)]
    all_to_all x2 -> x0, blocking collectives: 8.97 us -> none  [the longest x1 4.85 us: sent_to_all(): lax.all_to_all(jnp.broadcast_to(value[None], (size, *value.shape)), axis,...]
    all_to_all x4 -> x2, starting transfers between devices: 28.1 us -> 23.2 us  [the longest x1 13 us: local(): lax.all_to_all(far.reshape(KV_SIZE, LINES // 2, 2, 128), KV, 0, 0, tiled=...]
    unnamed x20 -> x4, local copies, waits for them, and re-layouts: 6.3 us -> 1.43 us
    dot_general x4 -> x0, matrix products: 3.9 us -> none  [the longest x1 1.5 us: local(): product = jnp.dot(normed, weights, preferred_element_type=jnp.float32)]
    gather x7 -> x0, local copies, waits for them, and re-layouts: 3.77 us -> none  [the longest x6 3.19 us: take_window(): kept_rows = jnp.take_along_axis(history, indices[:, :, None], axis=1)]
    all_to_all x2 -> x0, other arithmetic: 3.56 us -> none  [the longest x1 2.3 us: sent_and_summed_2(): lax.all_to_all(blocks, axis, split_axis=0, concat_axis=0, tiled=True)]
  transfers between devices with their start and end apart: 6 -> 2, of which waited for: 5 -> 2; matrix products, arithmetic and copies ran while one was open for 20% -> 0% of each run, Pallas kernels for 0% -> 13%
where the time goes in v1:
time: 56.6 us; the launch traced here: 56.2 us
  starting transfers between devices  23.2 us (41%)
  waiting for transfers between devices  14.6 us (26%)
  Pallas kernels  14.4 us (25%)
  between operations  2.6 us (5%)
  local copies, waits for them, and re-layouts  1.43 us (3%)
    all_to_all x1, waiting for transfers between devices, local(): lax.all_to_all(far.reshape(KV_SIZE, LINES // 2, 2, 128), KV, 0, 0, tiled=...  14 us
    all_to_all x1, starting transfers between devices, local(): lax.all_to_all(far.reshape(KV_SIZE, LINES // 2, 2, 128), KV, 0, 0, tiled=...  13 us
    all_to_all x1, starting transfers between devices, local(): arrived = lax.all_to_all(near, NEAR, 0, 0, tiled=True)  10.2 us
    pallas_call x1, Pallas kernels, local(): pl.pallas_call(prepare_body, out_shape=(shape((SEQS, HEAD, STATE), F32),...  4.94 us
    pallas_call x1, Pallas kernels, local(): pl.pallas_call(mix_body, out_shape=(shape((lines, 128), BF16), shape((7,...  2.84 us
    pallas_call x1, Pallas kernels, local(): pl.pallas_call(state_body, out_shape=shape((SEQS, PROPS + 1, 1, HEAD, STA...  2.55 us
    pallas_call x1, Pallas kernels, local(): pl.pallas_call(project_body, out_shape=shape((TP * NEAR_KV, 2 * TOKENS, 1...  2.31 us
    pallas_call x1, Pallas kernels, local(): pl.pallas_call(finish_body, out_shape=shape((TOKENS, TOKENS), BF16), in_s...  1.78 us
  transfers between devices with their start and end apart: 2, of which 2 were waited for; matrix products, arithmetic and copies ran while one was open for 0% of the time, Pallas kernels for 13%

profile of v1, /device:TPU:1, one launch (start us, length us, event | category | flops | bytes accessed | tf_op | source)
XLA Modules:
  0.0 56.2 jit_solution(13125872436781846902)
XLA Ops:
  0.6 2.3 %project.1 = bf16[16,64,128]{2,1,0:T(8,128)(2,1)} custom-call(s32[8]{0:T(128)} %accepted.5, bf16[128,1024]{1,0:T(8,128)(2,1)} %hidden.1, bf16[1024]{0:T(1024)(128)(2,1)} %gain.1, bf16[64,1024]{1,0:T(8,128)(2,1)} %bitcast.13, bf16[64,1024]{1,0:T(8,128)(2,1)} %bitcast.14, bf16[64,1024]{1,0:T(8,128)(2,1)} %bitcast.15, bf16[1,1024]{1,0:T(2,128)(2,1)} %bitcast.18, ...), custom_call_target="tpu_custom_call" | custom-call | tf_op jit(solution)/shard_map/project/pallas_call | solution.py:324
  2.9 10.2 %all-to-all-start = ((bf16[16,64,128]{2,1,0:T(8,128)(2,1)}), bf16[16,64,128]{2,1,0:T(8,128)(2,1)S(1)}, u32[]{:S(2)}, u32[]{:S(2)}) async-start(bf16[16,64,128]{2,1,0:T(8,128)(2,1)} %project.1), calls=%async_computation | async-start | bytes 524288 | tf_op jit(solution)/shard_map/near/all_to_all | solution.py:332
  15.1 4.9 %prepare.1 = (f32[8,64,128]{2,1,0:T(8,128)}, bf16[1280,256]{1,0:T(8,128)(2,1)}) custom-call(s32[8]{0:T(128)} %accepted.5, f32[8,5,1,64,128]{4,3,2,1,0:T(8,128)} %saved.1, bf16[64,4096]{1,0:T(8,128)(2,1)} %weight.1), custom_call_target="tpu_custom_call" | custom-call | flops 4000000 | bytes 3000000 | tf_op jit(solution)/shard_map/prepare/pallas_call | solution.py:334
  20.0 0.6 %all-to-all-done.arrived = bf16[16,64,128]{2,1,0:T(8,128)(2,1)S(1)} async-done(((bf16[16,64,128]{2,1,0:T(8,128)(2,1)}), bf16[16,64,128]{2,1,0:T(8,128)(2,1)S(1)}, u32[]{:S(2)}, u32[]{:S(2)}) %all-to-all-start) | async-done | bytes 262176 | tf_op jit(solution)/shard_map/near/all_to_all | solution.py:332
  20.7 0.0 copy-start.1
  20.7 0.7 %copy-done.1 = bf16[16,64,128]{2,1,0:T(8,128)(2,1)} copy-done((bf16[16,64,128]{2,1,0:T(8,128)(2,1)}, bf16[16,64,128]{2,1,0:T(8,128)(2,1)S(1)}, u32[]{:S(2)}) %copy-start.1) | copy-done | bytes 262168
  21.4 2.8 %mix.1 = (bf16[1280,128]{1,0:T(8,128)(2,1)}, bf16[7,8,64]{2,1,0:T(8,128)(2,1)}, bf16[7,8,64]{2,1,0:T(8,128)(2,1)}, f32[32,128]{1,0:T(8,128)}, f32[32,128]{1,0:T(8,128)}, /*index=5*/f32[32,128]{1,0:T(8,128)}) custom-call(s32[8]{0:T(128)} %accepted.5, f32[1]{0:T(128)S(6)} %copy.21.dt_bias, f32[1]{0:T(128)S(6)} %copy.22.decay_log, f32[1]{0:T(128)S(6)} %copy.23.skip_scale, ...), custom_call_target="tpu_custom_call" | custom-call | tf_op jit(solution)/shard_map/mix/pallas_call | solution.py:344
  24.2 13.0 %all-to-all-start.1 = ((bf16[128,5,2,128]{3,2,1,0:T(2,128)(2,1)}), bf16[128,5,2,128]{3,2,1,0:T(2,128)(2,1)S(1)}, u32[]{:S(2)}, u32[]{:S(2)}) async-start(bf16[128,5,2,128]{3,2,1,0:T(2,128)(2,1)} %bitcast.12), calls=%async_computation.1 | async-start | bytes 655360 | tf_op jit(solution)/shard_map/far/all_to_all | solution.py:374
  37.2 2.5 %states.1 = f32[8,5,1,64,128]{4,3,2,1,0:T(8,128)} custom-call(f32[32,128]{1,0:T(8,128)} %get-tuple-element.15.inputs, f32[32,128]{1,0:T(8,128)} %get-tuple-element.16.b_terms, f32[32,128]{1,0:T(8,128)} %get-tuple-element.17.decay, f32[8,64,128]{2,1,0:T(8,128)} %get-tuple-element.12.first_state), custom_call_target="tpu_custom_call" | custom-call | flops 4000000 | bytes 3000000 | tf_op jit(solution)/shard_map/states/pallas_call | solution.py:376
  39.7 14.0 %all-to-all-done.1 = bf16[128,5,2,128]{3,2,1,0:T(2,128)(2,1)S(1)} async-done(((bf16[128,5,2,128]{3,2,1,0:T(2,128)(2,1)}), bf16[128,5,2,128]{3,2,1,0:T(2,128)(2,1)S(1)}, u32[]{:S(2)}, u32[]{:S(2)}) %all-to-all-start.1) | async-done | bytes 327712 | tf_op jit(solution)/shard_map/far/all_to_all | solution.py:374
  53.7 0.0 copy-start
  53.7 0.7 %copy-done = bf16[128,5,2,128]{3,2,1,0:T(2,128)(2,1)} copy-done((bf16[128,5,2,128]{3,2,1,0:T(2,128)(2,1)}, bf16[128,5,2,128]{3,2,1,0:T(2,128)(2,1)S(1)}, u32[]{:S(2)}) %copy-start) | copy-done | bytes 327704
  54.5 1.8 %finish.1 = bf16[32,32]{1,0:T(8,128)(2,1)} custom-call(bf16[1280,128]{1,0:T(8,128)(2,1)} %bitcast.11), custom_call_target="tpu_custom_call" | custom-call | tf_op jit(solution)/shard_map/finish/pallas_call | solution.py:384
Async XLA Ops:
  2.9 17.7 %all-to-all-start = ((bf16[16,64,128]{2,1,0:T(8,128)(2,1)}), bf16[16,64,128]{2,1,0:T(8,128)(2,1)S(1)}, u32[]{:S(2)}, u32[]{:S(2)}) async-start(bf16[16,64,128]{2,1,0:T(8,128)(2,1)} %project.1), calls=%async_computation | async-start | bytes 524288 | tf_op jit(solution)/shard_map/near/all_to_all | solution.py:332
  20.7 0.7 %copy-start.1 = (bf16[16,64,128]{2,1,0:T(8,128)(2,1)}, bf16[16,64,128]{2,1,0:T(8,128)(2,1)S(1)}, u32[]{:S(2)}) copy-start(bf16[16,64,128]{2,1,0:T(8,128)(2,1)S(1)} %all-to-all-done.arrived) | copy-start | bytes 786436
  24.2 29.6 %all-to-all-start.1 = ((bf16[128,5,2,128]{3,2,1,0:T(2,128)(2,1)}), bf16[128,5,2,128]{3,2,1,0:T(2,128)(2,1)S(1)}, u32[]{:S(2)}, u32[]{:S(2)}) async-start(bf16[128,5,2,128]{3,2,1,0:T(2,128)(2,1)} %bitcast.12), calls=%async_computation.1 | async-start | bytes 655360 | tf_op jit(solution)/shard_map/far/all_to_all | solution.py:374
  53.7 0.7 %copy-start = (bf16[128,5,2,128]{3,2,1,0:T(2,128)(2,1)}, bf16[128,5,2,128]{3,2,1,0:T(2,128)(2,1)S(1)}, u32[]{:S(2)}) copy-start(bf16[128,5,2,128]{3,2,1,0:T(2,128)(2,1)S(1)} %all-to-all-done.1) | copy-start | bytes 983044

commit v2 on v1

--- a/solution.py
+++ b/solution.py
@@ -45,12 +45,10 @@
     return v / (1.0 + jnp.exp(-v))
 
 
-def accepted_column(accepted, shape):
-    rows = rows_of(shape)
-    column = jnp.zeros(shape, jnp.int32)
-    for s in range(SEQS):
-        column = jnp.where(rows == s, accepted[s], column)
-    return column
+def accepted_column(accepted):
+    line = jnp.broadcast_to(accepted[...].astype(F32)[None, :], (SEQS, SEQS))
+    own = lanes_of((SEQS, SEQS)) == rows_of((SEQS, SEQS))
+    return jnp.sum(jnp.where(own, line, 0.0), axis=1, keepdims=True)
 
 
 def kept_rows(history, column):
@@ -59,7 +57,7 @@
     for m in range(3):
         row = whole[m]
         for a in range(1, PROPS + 1):
-            row = jnp.where(column == a, whole[m + a], row)
+            row = jnp.where(column == float(a), whole[m + a], row)
         kept.append(row)
     return kept
 
@@ -81,7 +79,7 @@
     rows = rows_of((8, 128))
     upper = lanes_of((8, 128)) >= HEAD
     lines = jnp.where(rows == 4, dt_line, jnp.where(rows == 5, square_high, square_line - square_high))
-    column = accepted_column(accepted, (SEQS, HEAD))
+    column = accepted_column(accepted)
     empty = jnp.zeros((SEQS, HEAD), F32)
     extra = [jnp.concatenate([empty, row], axis=1) for row in kept_rows(bc_history, column)]
     taps = jnp.concatenate([bc_kernel[...].astype(F32), jnp.zeros((4, HEAD), F32)], axis=0)
@@ -96,27 +94,12 @@
             message[g * TP + j] = block
 
 
-def prepare_body(accepted, saved, weight, first_state, turned_weight, arrivals):
+def prepare_body(accepted, saved, first_state, arrivals):
     copies = [
         pltpu.make_async_copy(saved.at[s, accepted[s], 0], first_state.at[s], arrivals.at[s]) for s in range(SEQS)
     ]
     for copy in copies:
         copy.start()
-    gap = jnp.zeros((LINES - 8, 256), F32)
-
-    def turn(i, _):
-        block = weight[:, pl.ds(pl.multiple_of(i * 256, 256), 256)].astype(F32)
-        turned = jnp.transpose(block)
-        pieces = []
-        for d in range(8):
-            quarter = [turned[32 * d + 8 * q : 32 * d + 8 * q + 8] for q in range(4)]
-            pieces += [jnp.concatenate(quarter, axis=1), gap]
-        turned_weight[pl.ds(pl.multiple_of(i * 8 * LINES, 16), 8 * LINES), :] = jnp.concatenate(pieces, axis=0).astype(
-            BF16
-        )
-        return 0
-
-    lax.fori_loop(0, weight.shape[1] // 256, turn, 0)
     for copy in copies:
         copy.wait()
 
@@ -128,7 +111,7 @@
     skip_scale,
     arrived,
     first_state,
-    turned_weight,
+    weight,
     x_kernel,
     x_history,
     output_gain,
@@ -139,8 +122,6 @@
     b_out,
     decay_out,
     columns,
-    ordered,
-    square_rows,
 ):
     place = lax.axis_index(("yl", "c"))
     mine = lax.axis_index("tp")
@@ -161,12 +142,14 @@
     lined = jnp.where(rows == 5, jnp.broadcast_to(lax.rsqrt(mean + EPSILON), tile), ending)
     columns[...] = jnp.transpose(lined)[HEAD : HEAD + TOKENS]
     scale, step, cumulated = [], [], []
-    rate = jnp.exp(jnp.full((SEQS, 1), decay_log[0], F32))
+    bias = dt_bias[...].reshape(1, 1)
+    skip = skip_scale[...].reshape(1, 1)
+    rate = jnp.exp(decay_log[...].reshape(1, 1))
     total = jnp.zeros((SEQS, 1), F32)
     for t in range(PROPS):
         column = columns[pl.ds(t, SEQS, stride=PROPS), :]
         scale.append(column[:, 5:6])
-        raw = rounded(column[:, 5:6] * column[:, 4:5]) + dt_bias[0]
+        raw = rounded(column[:, 5:6] * column[:, 4:5]) + bias
         step.append(jnp.maximum(raw, 0.0) + jnp.log1p(jnp.exp(-jnp.abs(raw))))
         total = total - rate * step[t]
         cumulated.append(total)
@@ -200,7 +183,7 @@
 
     b_terms = terms(0, 1)
     c_terms = terms(2, 3)
-    column = accepted_column(accepted, (SEQS, HEAD))
+    column = accepted_column(accepted)
     kept = kept_rows(x_history, column)
     empty = jnp.zeros((SEQS, HEAD), F32)
     x_taps = jnp.concatenate([x_kernel[...].astype(F32), jnp.zeros((4, HEAD), F32)], axis=1)
@@ -208,6 +191,9 @@
     states = first_state[...].reshape(SEQS * HEAD, STATE).astype(BF16)
     read = dot_nt(jnp.concatenate(c_terms, axis=0).astype(BF16), states)
     gain = output_gain[...].astype(F32)
+    gain = jnp.concatenate([gain, gain], axis=1)
+    scaled = []
+    squares = jnp.zeros(tile, F32)
     for t in range(PROPS):
         picked = jnp.zeros(tile, F32)
         for k in range(SEQS // 2):
@@ -217,40 +203,43 @@
         for r in range(t + 1):
             product = jnp.sum(c_terms[t] * b_terms[r], axis=1, keepdims=True)
             output = output + (jnp.exp(cumulated[t] - cumulated[r]) * step[r] * product) * x_conv[r]
-        output = output + skip_scale[0] * x_conv[t]
+        output = output + skip * x_conv[t]
         gated = jnp.where(lower, output * silu(pltpu.roll(fresh[t], HEAD, 1)), 0.0)
         square = jnp.sum(gated * gated, axis=1, keepdims=True)
-        ordered[pl.ds(t, SEQS, stride=PROPS), :] = gated
-        square_rows[pl.ds(t, SEQS, stride=PROPS), :] = jnp.broadcast_to(square, tile)
+        scaled.append(jnp.where(lower, gated * gain, 0.0)[:, :HEAD])
+        squares = jnp.where(lanes // TOKENS == t, square, squares)
         inputs_out[8 * t : 8 * t + 8, :] = x_conv[t] * step[t]
         b_out[8 * t : 8 * t + 8, :] = b_terms[t]
         decay_out[8 * t : 8 * t + 8, :] = jnp.broadcast_to(jnp.exp(-rate * step[t]), tile)
-    scaled = ordered[...] * jnp.concatenate([gain, gain], axis=1)
-    scaled = scaled.astype(BF16)
-    moved = pltpu.roll(ordered[...], HEAD, 1) * jnp.concatenate([gain, gain], axis=1)
-    moved = moved.astype(BF16)
-    none = jnp.zeros((TOKENS, 128), BF16)
-    spread = jnp.concatenate(
-        [
-            jnp.concatenate([scaled, none], axis=1),
-            jnp.concatenate([moved, none], axis=1),
-            jnp.concatenate([none, scaled], axis=1),
-            jnp.concatenate([none, moved], axis=1),
-        ],
-        axis=0,
-    )
-    squares = square_rows[...]
-    square_line = jnp.transpose(jnp.concatenate([squares] * 4, axis=0))[0:1]
+    turns = []
+    for d in range(4):
+        turns += [row if d == 0 else pltpu.roll(row, 2 * d, 0) for row in scaled]
+    turns = jnp.concatenate(turns, axis=0).astype(BF16)
+    square_line = jnp.sum(jnp.where(lanes % TOKENS == rows, squares, 0.0), axis=0, keepdims=True)
     high = rounded(square_line)
-    low = square_line - high
-    period = 4 * LINES
-    spot = rows_of((period, 128)) % LINES
-    lines = jnp.where(spot == 8, high, jnp.where(spot == 9, low, 0.0))
-    part = 8 * period
-    lines = jnp.concatenate([lines] * 8, axis=0)
-    for i in range(turned_weight.shape[0] // part):
-        product = dot_nt(turned_weight[part * i : part * (i + 1), :], spread)
-        message[part * i : part * (i + 1), :] = (product + lines).astype(BF16)
+    lines = jnp.where(rows % 2 == 0, high, square_line - high)
+    quarter = lanes // TOKENS
+    for i in range(weight.shape[1] // 256):
+        product = jnp.dot(turns, weight[:, 256 * i : 256 * (i + 1)], preferred_element_type=F32)
+        pieces = []
+        for half in range(2):
+            block = product[:, 128 * half : 128 * (half + 1)]
+            spots = []
+            for d in range(4):
+                spot = None
+                for q in range(4):
+                    piece = block[32 * d + 8 * q : 32 * d + 8 * q + 8]
+                    piece = piece if q == d else pltpu.roll(piece, (32 * (q - d)) % 128, 1)
+                    spot = piece if q == 0 else jnp.where(quarter == q, piece, spot)
+                spots.append(spot)
+            pieces += [
+                spots[0],
+                jnp.where(rows < 2, lines, spots[1]),
+                jnp.where(rows < 2, spots[1], jnp.where(rows < 4, lines, spots[2])),
+                jnp.where(rows < 4, spots[2], jnp.where(rows < 6, lines, spots[3])),
+                jnp.where(rows < 6, spots[3], lines),
+            ]
+        message[80 * i : 80 * (i + 1), :] = jnp.concatenate(pieces, axis=0).astype(BF16)
     own_extra = tiles(arrived[place * TP + mine, 32:64, :].astype(F32))
     for m in range(3):
         x_window[m] = kept[m].astype(BF16)
@@ -272,7 +261,7 @@
             new_states[s, t + 1, 0] = state
 
 
-def finish_body(arrived, mixed, total):
+def finish_body(arrived, mixed, total, placed):
     step = 8 * LINES
     running = arrived[0:step, :].astype(F32)
     for i in range(1, arrived.shape[0] // step):
@@ -283,10 +272,14 @@
     for i in range(1, 8):
         summed = summed + total[LINES * i : LINES * i + 8, :]
         squares = squares + total[LINES * i + 8 : LINES * i + 10, :]
-    mean = (squares[0:1] + squares[1:2]) / INNER
-    summed = summed * lax.rsqrt(mean + EPSILON)
-    stacked = jnp.concatenate([summed] + [pltpu.roll(summed, 128 - 32 * q, 1) for q in range(1, 4)], axis=0)
-    mixed[...] = jnp.transpose(stacked)[:TOKENS].astype(BF16)
+    mean = jnp.broadcast_to((squares[0:1] + squares[1:2]) / INNER, (8, 128))
+    lanes = lanes_of((8, 128))
+    rows = rows_of((8, 128))
+    for t in range(PROPS):
+        own = jnp.sum(jnp.where(lanes == TOKENS * t + rows, mean, 0.0), axis=1, keepdims=True)
+        moved = summed if t == 0 else pltpu.roll(summed, 128 - TOKENS * t, 1)
+        placed[pl.ds(t, SEQS, stride=PROPS), :] = lax.rsqrt(own + EPSILON) * moved
+    mixed[...] = placed[...][:, :TOKENS].astype(BF16)
 
 
 def smem():
@@ -295,6 +288,10 @@
 
 def vmem():
     return pl.BlockSpec(memory_space=pltpu.VMEM)
+
+
+def near_memory(value):
+    return pltpu.with_memory_space_constraint(value, pltpu.VMEM)
 
 
 def local(
@@ -317,47 +314,44 @@
     accepted,
 ):
     shape = jax.ShapeDtypeStruct
+    held = pltpu.VMEM
     lines = KV_SIZE * LINES
     x_rows = jnp.transpose(x_history, (1, 0, 2))
     bc_rows = jnp.transpose(bc_history, (1, 0, 2))
     with jax.named_scope("project"):
         near = pl.pallas_call(
             project_body,
-            out_shape=shape((TP * NEAR_KV, 2 * TOKENS, 128), BF16),
-            in_specs=[smem()] + [vmem()] * 8,
+            out_shape=held((TP * NEAR_KV, 2 * TOKENS, 128), BF16),
+            in_specs=[vmem()] * 9,
             out_specs=vmem(),
             scratch_shapes=[pltpu.VMEM((128, 128), F32), pltpu.VMEM((128, 128), F32)],
         )(accepted, hidden, input_gain, x_weight.T, z_weight.T, bc_weight.T, dt_weight.T, bc_rows, bc_kernel)
     with jax.named_scope("near"):
-        arrived = lax.all_to_all(near, NEAR, 0, 0, tiled=True)
+        arrived = near_memory(lax.all_to_all(near, NEAR, 0, 0, tiled=True))
     with jax.named_scope("prepare"):
-        first_state, turned_weight = pl.pallas_call(
+        first_state = pl.pallas_call(
             prepare_body,
-            out_shape=(shape((SEQS, HEAD, STATE), F32), shape((lines, 256), BF16)),
-            in_specs=[smem(), pl.BlockSpec(memory_space=pl.ANY), vmem()],
-            out_specs=(vmem(), vmem()),
+            out_shape=held((SEQS, HEAD, STATE), F32),
+            in_specs=[smem(), pl.BlockSpec(memory_space=pl.ANY)],
+            out_specs=vmem(),
             scratch_shapes=[pltpu.SemaphoreType.DMA((SEQS,))],
             cost_estimate=pl.CostEstimate(flops=4_000_000, bytes_accessed=3_000_000, transcendentals=0),
-        )(accepted, saved_states, output_weight)
-        gain_row = output_gain.reshape(1, HEAD)
+        )(accepted, saved_states)
+        first_state = near_memory(first_state)
     with jax.named_scope("mix"):
         far, x_window, bc_window, inputs, b_terms, decay = pl.pallas_call(
             mix_body,
             out_shape=(
-                shape((lines, 128), BF16),
+                held((lines, 128), BF16),
                 shape((7, SEQS, HEAD), BF16),
                 shape((7, SEQS, HEAD), BF16),
-                shape((TOKENS, 128), F32),
-                shape((TOKENS, 128), F32),
-                shape((TOKENS, 128), F32),
+                held((TOKENS, 128), F32),
+                held((TOKENS, 128), F32),
+                held((TOKENS, 128), F32),
             ),
-            in_specs=[smem()] * 4 + [vmem()] * 6,
+            in_specs=[vmem()] * 10,
             out_specs=(vmem(),) * 6,
-            scratch_shapes=[
-                pltpu.VMEM((TOKENS, 8), F32),
-                pltpu.VMEM((TOKENS, 128), F32),
-                pltpu.VMEM((TOKENS, 128), F32),
-            ],
+            scratch_shapes=[pltpu.VMEM((TOKENS, 8), F32)],
         )(
             accepted,
             dt_bias,
@@ -365,13 +359,14 @@
             skip_scale,
             arrived,
             first_state,
-            turned_weight,
+            near_memory(output_weight),
             x_kernel,
             x_rows,
-            gain_row,
+            output_gain.reshape(1, HEAD),
         )
     with jax.named_scope("far"):
         landed = lax.all_to_all(far.reshape(KV_SIZE, LINES // 2, 2, 128), KV, 0, 0, tiled=True)
+        landed = near_memory(landed.reshape(lines, 128))
     with jax.named_scope("states"):
         new_states = pl.pallas_call(
             state_body,
@@ -379,15 +374,15 @@
             in_specs=[vmem()] * 4,
             out_specs=vmem(),
             cost_estimate=pl.CostEstimate(flops=4_000_000, bytes_accessed=3_000_000, transcendentals=0),
-        )(inputs, b_terms, decay, first_state)
+        )(near_memory(inputs), near_memory(b_terms), near_memory(decay), first_state)
     with jax.named_scope("finish"):
         mixed = pl.pallas_call(
             finish_body,
             out_shape=shape((TOKENS, TOKENS), BF16),
             in_specs=[vmem()],
             out_specs=vmem(),
-            scratch_shapes=[pltpu.VMEM((8 * LINES, 128), F32)],
-        )(landed.reshape(lines, 128))
+            scratch_shapes=[pltpu.VMEM((8 * LINES, 128), F32), pltpu.VMEM((TOKENS, 128), F32)],
+        )(landed)
     return (mixed, new_states, jnp.transpose(x_window, (1, 0, 2)), jnp.transpose(bc_window, (1, 0, 2)))
 
 

time: 56.6 us -> 54 us (0.954)
  Pallas kernels: 14.4 us -> 8.77 us
  waiting for transfers between devices: 14.6 us -> 19 us
  local copies, waits for them, and re-layouts: 1.43 us -> 0.01 us
    pallas_call x3, Pallas kernels: 10.1 us -> 6.46 us  [the longest x1 2.48 us: local(): pl.pallas_call(mix_body, out_shape=(held((lines, 128), BF16), shape((7, S...]
    all_to_all x1, waiting for transfers between devices: 0.63 us -> 3.96 us  [local(): arrived = near_memory(lax.all_to_all(near, NEAR, 0, 0, tiled=True))]
    unnamed x4 -> x2, local copies, waits for them, and re-layouts: 1.43 us -> 0.01 us
    pallas_call x1, Pallas kernels: 1.78 us -> 0.76 us  [local(): pl.pallas_call(finish_body, out_shape=shape((TOKENS, TOKENS), BF16), in_s...]
    pallas_call x1, Pallas kernels: 2.55 us -> 1.54 us  [local(): pl.pallas_call(state_body, out_shape=shape((SEQS, PROPS + 1, 1, HEAD, STA...]
    all_to_all x1, waiting for transfers between devices: 14 us -> 15 us  [local(): lax.all_to_all(far.reshape(KV_SIZE, LINES // 2, 2, 128), KV, 0, 0, tiled=...]
  transfers between devices with their start and end apart: 2 -> 2, of which waited for: 2 -> 2; matrix products, arithmetic and copies ran while one was open for 0% -> 0% of each run, Pallas kernels for 13% -> 6%
where the time goes in v2:
time: 54 us; the launch traced here: 53.5 us
  starting transfers between devices  23.2 us (43%)
  waiting for transfers between devices  19 us (35%)
  Pallas kernels  8.77 us (16%)
  between operations  2.61 us (5%)
    all_to_all x1, waiting for transfers between devices, local(): lax.all_to_all(far.reshape(KV_SIZE, LINES // 2, 2, 128), KV, 0, 0, tiled=...  15 us
    all_to_all x1, starting transfers between devices, local(): lax.all_to_all(far.reshape(KV_SIZE, LINES // 2, 2, 128), KV, 0, 0, tiled=...  13 us
    all_to_all x1, starting transfers between devices, local(): arrived = near_memory(lax.all_to_all(near, NEAR, 0, 0, tiled=True))  10.2 us
    all_to_all x1, waiting for transfers between devices, local(): arrived = near_memory(lax.all_to_all(near, NEAR, 0, 0, tiled=True))  3.96 us
    pallas_call x1, Pallas kernels, local(): pl.pallas_call(mix_body, out_shape=(held((lines, 128), BF16), shape((7, S...  2.48 us
    pallas_call x1, Pallas kernels, local(): pl.pallas_call(project_body, out_shape=held((TP * NEAR_KV, 2 * TOKENS, 12...  2.37 us
    pallas_call x1, Pallas kernels, local(): pl.pallas_call(prepare_body, out_shape=held((SEQS, HEAD, STATE), F32), in...  1.61 us
    pallas_call x1, Pallas kernels, local(): pl.pallas_call(state_body, out_shape=shape((SEQS, PROPS + 1, 1, HEAD, STA...  1.54 us
  transfers between devices with their start and end apart: 2, of which 2 were waited for; matrix products, arithmetic and copies ran while one was open for 0% of the time, Pallas kernels for 6%

profile of v2, /device:TPU:1, one launch (start us, length us, event | category | flops | bytes accessed | tf_op | source)
XLA Modules:
  0.0 53.5 jit_solution(2462935866568395457)
XLA Ops:
  0.6 0.0 copy-start
  0.6 2.4 %project.1 = bf16[16,64,128]{2,1,0:T(8,128)(2,1)} custom-call(s32[8]{0:T(128)} %accepted.5, bf16[128,1024]{1,0:T(8,128)(2,1)} %hidden.1, bf16[1024]{0:T(1024)(128)(2,1)} %gain.1, bf16[64,1024]{1,0:T(8,128)(2,1)} %bitcast.12, bf16[64,1024]{1,0:T(8,128)(2,1)} %bitcast.13, bf16[64,1024]{1,0:T(8,128)(2,1)} %bitcast.14, bf16[1,1024]{1,0:T(2,128)(2,1)} %bitcast.17, ...), custom_call_target="tpu_custom_call" | custom-call | tf_op jit(solution)/shard_map/project/pallas_call | solution.py:322
  3.0 10.2 %all-to-all-start = ((bf16[16,64,128]{2,1,0:T(8,128)(2,1)}), bf16[16,64,128]{2,1,0:T(8,128)(2,1)S(1)}, u32[]{:S(2)}, u32[]{:S(2)}) async-start(bf16[16,64,128]{2,1,0:T(8,128)(2,1)} %project.1), calls=%async_computation | async-start | bytes 524288 | tf_op jit(solution)/shard_map/near/all_to_all | solution.py:330
  15.1 1.6 %prepare.1.first_state = f32[8,64,128]{2,1,0:T(8,128)S(1)} custom-call(s32[8]{0:T(128)} %accepted.5, f32[8,5,1,64,128]{4,3,2,1,0:T(8,128)} %saved.1), custom_call_target="tpu_custom_call" | custom-call | flops 4000000 | bytes 3000000 | tf_op jit(solution)/shard_map/prepare/pallas_call | solution.py:332
  16.8 4.0 %all-to-all-done.arrived = bf16[16,64,128]{2,1,0:T(8,128)(2,1)S(1)} async-done(((bf16[16,64,128]{2,1,0:T(8,128)(2,1)}), bf16[16,64,128]{2,1,0:T(8,128)(2,1)S(1)}, u32[]{:S(2)}, u32[]{:S(2)}) %all-to-all-start) | async-done | bytes 262176 | tf_op jit(solution)/shard_map/near/all_to_all | solution.py:330
  20.7 0.0 copy-done
  20.7 2.5 %mix.1 = (bf16[1280,128]{1,0:T(8,128)(2,1)}, bf16[7,8,64]{2,1,0:T(8,128)(2,1)}, bf16[7,8,64]{2,1,0:T(8,128)(2,1)}, f32[32,128]{1,0:T(8,128)S(1)}, f32[32,128]{1,0:T(8,128)S(1)}, /*index=5*/f32[32,128]{1,0:T(8,128)S(1)}) custom-call(s32[8]{0:T(128)} %accepted.5, f32[1]{0:T(128)S(6)} %copy.21.dt_bias, f32[1]{0:T(128)S(6)} %copy.22.decay_log, ...), custom_call_target="tpu_custom_call" | custom-call | tf_op jit(solution)/shard_map/mix/pallas_call | solution.py:342
  23.2 13.0 %all-to-all-start.1 = ((bf16[128,5,2,128]{3,2,1,0:T(2,128)(2,1)}), bf16[128,5,2,128]{3,2,1,0:T(2,128)(2,1)S(1)}, u32[]{:S(2)}, u32[]{:S(2)}) async-start(bf16[128,5,2,128]{3,2,1,0:T(2,128)(2,1)} %bitcast.7), calls=%async_computation.1 | async-start | bytes 655360 | tf_op jit(solution)/shard_map/far/all_to_all | solution.py:368
  36.2 1.5 %states.1 = f32[8,5,1,64,128]{4,3,2,1,0:T(8,128)} custom-call(f32[32,128]{1,0:T(8,128)S(1)} %get-tuple-element.11.inputs, f32[32,128]{1,0:T(8,128)S(1)} %get-tuple-element.12.b_terms, f32[32,128]{1,0:T(8,128)S(1)} %get-tuple-element.13.decay, f32[8,64,128]{2,1,0:T(8,128)S(1)} %prepare.1.first_state), custom_call_target="tpu_custom_call" | custom-call | flops 4000000 | bytes 3000000 | tf_op jit(solution)/shard_map/states/pallas_call | solution.py:371
  37.8 15.0 %all-to-all-done.1 = bf16[128,5,2,128]{3,2,1,0:T(2,128)(2,1)S(1)} async-done(((bf16[128,5,2,128]{3,2,1,0:T(2,128)(2,1)}), bf16[128,5,2,128]{3,2,1,0:T(2,128)(2,1)S(1)}, u32[]{:S(2)}, u32[]{:S(2)}) %all-to-all-start.1) | async-done | bytes 327712 | tf_op jit(solution)/shard_map/far/all_to_all | solution.py:368
  52.8 0.8 %finish.1 = bf16[32,32]{1,0:T(8,128)(2,1)} custom-call(bf16[1280,128]{1,0:T(8,128)(2,1)S(1)} %bitcast.11), custom_call_target="tpu_custom_call" | custom-call | tf_op jit(solution)/shard_map/finish/pallas_call | solution.py:379
Async XLA Ops:
  0.6 20.1 %copy-start = (bf16[64,4096]{1,0:T(8,128)(2,1)S(1)}, bf16[64,4096]{1,0:T(8,128)(2,1)}, u32[]{:S(2)}) copy-start(bf16[64,4096]{1,0:T(8,128)(2,1)} %weight.1) | copy-start | bytes 1572868
  3.0 17.7 %all-to-all-start = ((bf16[16,64,128]{2,1,0:T(8,128)(2,1)}), bf16[16,64,128]{2,1,0:T(8,128)(2,1)S(1)}, u32[]{:S(2)}, u32[]{:S(2)}) async-start(bf16[16,64,128]{2,1,0:T(8,128)(2,1)} %project.1), calls=%async_computation | async-start | bytes 524288 | tf_op jit(solution)/shard_map/near/all_to_all | solution.py:330
  23.2 29.6 %all-to-all-start.1 = ((bf16[128,5,2,128]{3,2,1,0:T(2,128)(2,1)}), bf16[128,5,2,128]{3,2,1,0:T(2,128)(2,1)S(1)}, u32[]{:S(2)}, u32[]{:S(2)}) async-start(bf16[128,5,2,128]{3,2,1,0:T(2,128)(2,1)} %bitcast.7), calls=%async_computation.1 | async-start | bytes 655360 | tf_op jit(solution)/shard_map/far/all_to_all | solution.py:368

commit v3 on v2

v3 whole, which is shorter than its diff:
```python
import jax
import jax.numpy as jnp
from jax import lax
from jax.experimental import pallas as pl
from jax.experimental.pallas import tpu as pltpu
from jax.sharding import Mesh
from jax.sharding import PartitionSpec as P


D = 4096
PROPS = 4
INNER = 8192
KV = ("z", "yh", "yl", "c")
NEAR = ("yl", "c", "tp")
EPSILON = 1e-05
TP = 4
NEAR_KV = 4
KV_SIZE = 128
SEQS = 8
HALF = 4
TOKENS = 32
HEAD = 64
STATE = 128
LINES = 6
TILE = (8, 128)
SMALL = 64

F32 = jnp.float32
BF16 = jnp.bfloat16


def rounded(value):
    return value.astype(BF16).astype(F32)


def lanes_of(shape):
    return lax.broadcasted_iota(jnp.int32, shape, len(shape) - 1)


def rows_of(shape):
    return lax.broadcasted_iota(jnp.int32, shape, len(shape) - 2)


def dot_nt(a, b):
    return lax.dot_general(a, b, (((1,), (1,)), ((), ())), preferred_element_type=F32)


def silu(v):
    return v / (1.0 + jnp.exp(-v))


def softplus(v):
    return jnp.maximum(v, 0.0) + jnp.log1p(jnp.exp(-jnp.abs(v)))


def tiles(value):
    return [value[8 * i : 8 * i + 8] for i in range(value.shape[0] // 8)]


def swapped(tile):
    return pltpu.roll(tile, HEAD, 1)


def turned_half(tile):
    return pltpu.roll(tile, HALF, 0)


def widened(tile):
    return jnp.concatenate([tile, jnp.zeros(tile.shape, tile.dtype)], axis=1)


def kept_rows(history, accepted):
    rows = rows_of((SEQS, HEAD))
    column = jnp.zeros((SEQS, HEAD), jnp.int32)
    for s in range(SEQS):
        column = jnp.where(rows == s, accepted[s], column)
    whole = [history[i].astype(F32) for i in range(7)]
    kept = []
    for m in range(3):
        row = whole[m]
        for a in range(1, PROPS + 1):
            row = jnp.where(column == a, whole[m + a], row)
        kept.append(row)
    return kept


def convolved(window, taps):
    results = []
    for t in range(PROPS):
        running = window[t] * taps[0]
        for j in range(1, 4):
            running = running + window[t + j] * taps[j]
        results.append(silu(running))
    return results


def three_terms(value, shape):
    value = jnp.broadcast_to(value, shape)
    high = rounded(value)
    middle = rounded(value - high)
    lanes = lanes_of(shape)
    low = value - high - middle
    return jnp.where(lanes == HEAD, high, jnp.where(lanes == HEAD + 1, middle, jnp.where(lanes == HEAD + 2, low, 0.0)))


def project_body(
    accepted,
    saved,
    hidden,
    gain,
    x_weight,
    z_weight,
    bc_weight,
    dt_weight,
    bc_history,
    bc_kernel,
    message,
    first_state,
    first,
    second,
    arrivals,
):
    copies = [
        pltpu.make_async_copy(saved.at[s, accepted[s], 0], first_state.at[s], arrivals.at[s]) for s in range(SEQS)
    ]
    for copy in copies:
        copy.start()
    wide = hidden[...].astype(F32)
    scaled = (wide * gain[...].astype(F32)[None, :]).astype(BF16)
    squares = jnp.sum(wide * wide, axis=1, keepdims=True)
    dt_rows = jnp.broadcast_to(dt_weight[...], (HEAD, dt_weight.shape[1]))
    first[...] = dot_nt(scaled, jnp.concatenate([x_weight[...], z_weight[...]], axis=0))
    last = dot_nt(scaled, jnp.concatenate([bc_weight[...], dt_rows], axis=0))
    second[...] = last
    turned = jnp.transpose(jnp.where(lanes_of((128, 128)) == HEAD + 1, squares, last))
    dt_line = jnp.broadcast_to(turned[HEAD : HEAD + 1], TILE)
    square_line = jnp.broadcast_to(turned[HEAD + 1 : HEAD + 2], TILE)
    square_high = rounded(square_line)
    rows = rows_of(TILE)
    upper = lanes_of(TILE) >= HEAD
    lines = jnp.where(rows == 4, dt_line, jnp.where(rows == 5, square_high, square_line - square_high))
    empty = jnp.zeros((SEQS, HEAD), F32)
    extra = [jnp.concatenate([empty, row], axis=1) for row in kept_rows(bc_history, accepted)]
    taps = jnp.concatenate([bc_kernel[...].astype(F32), jnp.zeros((4, HEAD), F32)], axis=0)
    taps = jnp.concatenate([empty, taps], axis=1)
    for j in range(TP):
        top = [first[pl.ds(TOKENS * j + t, SEQS, stride=PROPS), :] for t in range(PROPS)]
        low = [second[pl.ds(TOKENS * j + t, SEQS, stride=PROPS), :] for t in range(PROPS)]
        ending = jnp.where(rows < 4, taps, pltpu.roll(lines, (64 - 32 * j) % 128, 1))
        low = [jnp.where(upper, e, v) for e, v in zip([*extra, ending], low)]
        block = jnp.concatenate(top + low, axis=0).astype(BF16)
        for g in range(NEAR_KV):
            message[g * TP + j] = block
    for copy in copies:
        copy.wait()


def pack_body(
    accepted,
    dt_bias,
    decay_log,
    skip_scale,
    first_state,
    weight,
    x_history,
    x_kernel,
    output_gain,
    kept_pack,
    sent,
):
    core = lax.axis_index("c")
    rows = rows_of(TILE)
    terms = [three_terms(number[0], TILE) for number in (dt_bias, decay_log, skip_scale)]
    gain_row = jnp.concatenate([jnp.zeros((1, HEAD), F32), output_gain[...].astype(F32)], axis=1)
    kernel = x_kernel[...].astype(F32)
    small = [widened(row) for row in kept_rows(x_history, accepted)]
    small = [jnp.where(core == 1, turned_half(tile), tile) for tile in small]
    small += [jnp.broadcast_to(widened(kernel[j : j + 1]), TILE) for j in range(4)]
    small = [small[0] + gain_row] + [a + b for a, b in zip(small[1:4], terms)] + small[4:]
    small.append(jnp.zeros(TILE, F32))
    kept_pack[0:SMALL, :] = jnp.concatenate([jnp.where(rows < HALF, tile, 0.0) for tile in small], axis=0).astype(BF16)
    kept_pack[SMALL:, :] = first_state[pl.ds(HALF * core, HALF)].reshape(HALF * HEAD, STATE).astype(BF16)
    sent[0:HEAD, :] = weight[...]
    small = [jnp.where(rows < HALF, 0.0, tile) for tile in small]
    states = first_state[pl.ds(HALF - HALF * core, HALF)].reshape(HALF * HEAD, STATE)
    blocks = [jnp.concatenate(small[2 * i : 2 * i + 2], axis=0) for i in range(SMALL // 16)]
    blocks += [states[16 * i : 16 * i + 16] for i in range(HALF * HEAD // 16)]
    blocks += [jnp.zeros((16, 128), F32)] * (weight.shape[1] // 128 - len(blocks))
    for i, block in enumerate(blocks):
        sent[HEAD : HEAD + 16, 128 * i : 128 * i + 128] = block.astype(BF16)


def summed_over_tp(arrived, place, start):
    total = arrived[place * TP, start : 2 * TOKENS, :].astype(F32)
    for k in range(1, TP):
        total = total + arrived[place * TP + k, start : 2 * TOKENS, :].astype(F32)
    return tiles(total)


def scale_line(ending):
    return lax.rsqrt((ending[5:6] + ending[6:7]) / D + EPSILON)


def mix_body(arrived, kept_pack, got, weight, message, columns):
    core = lax.axis_index("c")
    pair = lax.axis_index("yl") * 2
    mine = lax.axis_index("tp")
    lanes = lanes_of(TILE)
    rows = rows_of(TILE)
    lower = lanes < HEAD
    first_rows = rows < HALF
    second_core = core == 1

    def halves(own, other):
        own = jnp.where(second_core, turned_half(own), own)
        other = jnp.where(second_core, other, turned_half(other))
        return jnp.where(rows_of(own.shape) < HALF, own, other)

    own = summed_over_tp(arrived, pair + core, 0)
    other = summed_over_tp(arrived, pair + 1 - core, 0)
    got_small = [got[HEAD : HEAD + 16, 128 * i : 128 * i + 128] for i in range(SMALL // 16)]
    small = tiles(kept_pack[0:SMALL, :].astype(F32) + jnp.concatenate(got_small, axis=0).astype(F32))
    gain = swapped(small[0])
    bias, decay, skip = [
        tile[:, HEAD : HEAD + 1] + tile[:, HEAD + 1 : HEAD + 2] + tile[:, HEAD + 2 : HEAD + 3] for tile in small[1:4]
    ]
    ending = own[7]
    lined = jnp.where(rows == 0, jnp.broadcast_to(scale_line(ending), TILE), ending)
    lined = jnp.where(rows == 1, jnp.broadcast_to(other[7][4:5], TILE), lined)
    columns[...] = jnp.transpose(lined)[HEAD : HEAD + TOKENS]
    rate = jnp.exp(decay)
    scale, step, cumulated = [], [], []
    total = jnp.zeros((SEQS, 1), F32)
    for t in range(PROPS):
        column = columns[pl.ds(t, SEQS, stride=PROPS), :]
        column = halves(column, column)
        scale.append(column[:, 0:1])
        raw = jnp.where(rows_of((SEQS, 1)) < HALF, column[:, 4:5], column[:, 1:2])
        step.append(softplus(rounded(scale[t] * raw) + bias))
        total = total - rate * step[t]
        cumulated.append(total)
    fresh = [rounded(scale[t] * halves(own[t], other[t])) for t in range(PROPS)]
    sums, extras = [], []
    for g in range(NEAR_KV):
        sums.append(summed_over_tp(arrived, g, TOKENS))
        extras.append(tiles(arrived[g * TP + mine, TOKENS : 2 * TOKENS, :].astype(F32)))

    def terms(left, right):
        window = [jnp.where(lower, swapped(extras[left][m]), extras[right][m]) for m in range(4)]
        new = [jnp.where(lower, sums[left][t], swapped(sums[right][t])) for t in range(PROPS)]
        taps = [window[3][j : j + 1] for j in range(4)]
        window = [halves(tile, tile) for tile in window[:3]]
        return convolved(window + [rounded(scale[t] * halves(new[t], new[t])) for t in range(PROPS)], taps)

    b_terms = terms(0, 1)
    c_terms = terms(2, 3)
    x_conv = convolved(small[0:3] + fresh, small[3:7])
    spans = range(SMALL // 16, (SMALL + HALF * HEAD) // 16)
    got_states = [got[HEAD : HEAD + 16, 128 * i : 128 * i + 128] for i in spans]
    states = jnp.concatenate([kept_pack[SMALL:, :], *got_states], axis=0)
    read = dot_nt(jnp.concatenate(c_terms, axis=0).astype(BF16), states)
    scaled = []
    squares = jnp.zeros(TILE, F32)
    quarter = lanes // TOKENS
    for t in range(PROPS):
        picked = jnp.zeros(TILE, F32)
        for k in range(SEQS // 2):
            picked = jnp.where(rows // 2 == k, read[8 * t : 8 * t + 8, 128 * k : 128 * k + 128], picked)
        picked = jnp.where(rows % 2 == 0, picked, swapped(picked))
        output = jnp.exp(cumulated[t]) * picked
        for r in range(t + 1):
            product = jnp.sum(c_terms[t] * b_terms[r], axis=1, keepdims=True)
            output = output + (jnp.exp(cumulated[t] - cumulated[r]) * step[r] * product) * x_conv[r]
        output = output + skip * x_conv[t]
        gated = output * silu(swapped(fresh[t]))
        both = jnp.where(lower, gated, swapped(turned_half(gated)))
        squares = jnp.where(quarter == t, jnp.sum(both * both, axis=1, keepdims=True), squares)
        gains = jnp.where(lower, gain, swapped(turned_half(gain)))
        scaled.append(both * gains)
    turns = []
    for d in range(4):
        turns += [row if d == 0 else pltpu.roll(row, 8 - 2 * d, 0) for row in scaled]
    turns = jnp.concatenate(turns, axis=0).astype(BF16)
    spot = jnp.where(first_rows & (lanes % TOKENS == rows), squares, 0.0)
    square_line = jnp.sum(spot, axis=0, keepdims=True)
    high = rounded(square_line)
    lines = jnp.where(rows % 2 == 0, high, square_line - high)
    for i in range(weight.shape[1] // 256):
        cut = slice(256 * i, 256 * (i + 1))
        both_weights = jnp.concatenate([weight[:, cut], got[0:HEAD, cut]], axis=0)
        product = jnp.dot(turns, both_weights, preferred_element_type=F32)
        pieces = []
        for half in range(2):
            block = product[:, 128 * half : 128 * (half + 1)]
            spots = []
            for d in range(4):
                spot = None
                for t in range(PROPS):
                    piece = block[32 * d + 8 * t : 32 * d + 8 * t + 8]
                    piece = piece if t == d else pltpu.roll(piece, (32 * (t - d)) % 128, 1)
                    spot = piece if t == 0 else jnp.where(quarter == t, piece, spot)
                spots.append(spot)
            pieces += [
                jnp.where(rows < 4, spots[0], jnp.where(rows < 6, lines, spots[1])),
                jnp.where(rows < 2, spots[1], jnp.where(rows < 4, lines, spots[2])),
                jnp.where((rows >= 2) & (rows < 6), spots[3], lines),
            ]
        message[48 * i : 48 * (i + 1), :] = jnp.concatenate(pieces, axis=0).astype(BF16)


def state_body(
    accepted,
    dt_bias,
    decay_log,
    arrived,
    first_state,
    x_kernel,
    x_history,
    new_states,
    x_window,
    bc_window,
    columns,
):
    place = lax.axis_index(("yl", "c"))
    mine = lax.axis_index("tp")
    lanes = lanes_of(TILE)
    lower = lanes < HEAD
    own = summed_over_tp(arrived, place, 0)
    ending = own[7]
    lined = jnp.where(rows_of(TILE) == 0, jnp.broadcast_to(scale_line(ending), TILE), ending)
    columns[...] = jnp.transpose(lined)[HEAD : HEAD + TOKENS]
    bias = dt_bias[0]
    rate = jnp.exp(jnp.full((SEQS, 1), decay_log[0], F32))
    scale, step = [], []
    for t in range(PROPS):
        column = columns[pl.ds(t, SEQS, stride=PROPS), :]
        scale.append(column[:, 0:1])
        step.append(softplus(rounded(scale[t] * column[:, 4:5]) + bias))
    fresh = [rounded(scale[t] * own[t]) for t in range(PROPS)]
    sums = [summed_over_tp(arrived, g, TOKENS) for g in range(2)]
    extras = [tiles(arrived[g * TP + mine, TOKENS : 2 * TOKENS, :].astype(F32)) for g in range(2)]
    window = [jnp.where(lower, swapped(extras[0][m]), extras[1][m]) for m in range(4)]
    new = [rounded(scale[t] * jnp.where(lower, sums[0][t], swapped(sums[1][t]))) for t in range(PROPS)]
    b_terms = convolved(window[:3] + new, [window[3][j : j + 1] for j in range(4)])
    kept = kept_rows(x_history, accepted)
    kernel = widened(x_kernel[...].astype(F32))
    x_conv = convolved([widened(row) for row in kept] + fresh, [kernel[j : j + 1] for j in range(4)])
    inputs = [x_conv[t] * step[t] for t in range(PROPS)]
    turned = jnp.transpose(jnp.concatenate(inputs + [jnp.zeros((128 - TOKENS, 128), F32)], axis=0))[:HEAD]
    decay = [jnp.broadcast_to(jnp.exp(-rate * step[t]), TILE) for t in range(PROPS)]
    for s in range(SEQS):
        state = first_state[s]
        new_states[s, 0, 0] = state
        for t in range(PROPS):
            at = 8 * t + s
            state = state * decay[t][s : s + 1, :] + turned[:, at : at + 1] * b_terms[t][s : s + 1, :]
            new_states[s, t + 1, 0] = state
    own_extra = tiles(arrived[place * TP + mine, TOKENS : 2 * TOKENS, :].astype(F32))
    for m in range(3):
        x_window[m] = kept[m].astype(BF16)
        bc_window[m] = swapped(own_extra[m])[:, :HEAD].astype(BF16)
    for t in range(PROPS):
        x_window[3 + t] = fresh[t][:, :HEAD].astype(BF16)
        bc_window[3 + t] = (scale[t] * own[4 + t])[:, :HEAD].astype(BF16)


def finish_body(arrived, mixed, total, placed):
    step = 8 * LINES
    running = arrived[0:step, :].astype(F32)
    for i in range(1, arrived.shape[0] // step):
        running = running + arrived[step * i : step * (i + 1), :].astype(F32)
    total[...] = running
    sums = []
    for c in range(2):
        start = LINES * c
        part = total[start : start + LINES, :]
        for i in range(1, 4):
            part = part + total[2 * LINES * i + start : 2 * LINES * i + start + LINES, :]
        sums.append(part)
    summed = jnp.concatenate([part[:HALF] for part in sums], axis=0)
    means = [jnp.broadcast_to((part[4:5] + part[5:6]) / INNER, (HALF, 128)) for part in sums]
    mean = jnp.concatenate(means, axis=0)
    lanes = lanes_of(TILE)
    rows = rows_of(TILE)
    for t in range(PROPS):
        own = jnp.sum(jnp.where(lanes == TOKENS * t + rows % HALF, mean, 0.0), axis=1, keepdims=True)
        moved = summed if t == 0 else pltpu.roll(summed, 128 - TOKENS * t, 1)
        placed[pl.ds(t, SEQS, stride=PROPS), :] = lax.rsqrt(own + EPSILON) * moved
    mixed[...] = placed[...][:, :TOKENS].astype(BF16)


def smem():
    return pl.BlockSpec(memory_space=pltpu.SMEM)


def vmem():
    return pl.BlockSpec(memory_space=pltpu.VMEM)


def far_memory():
    return pl.BlockSpec(memory_space=pltpu.HBM)


def near_memory(value):
    return pltpu.with_memory_space_constraint(value, pltpu.VMEM)


def local(
    hidden,
    input_gain,
    x_weight,
    z_weight,
    bc_weight,
    dt_weight,
    x_kernel,
    bc_kernel,
    dt_bias,
    decay_log,
    skip_scale,
    output_gain,
    output_weight,
    saved_states,
    x_history,
    bc_history,
    accepted,
):
    shape = jax.ShapeDtypeStruct
    held = pltpu.VMEM
    lines = KV_SIZE * LINES
    x_rows = jnp.transpose(x_history, (1, 0, 2))
    bc_rows = jnp.transpose(bc_history, (1, 0, 2))
    pack_rows = SMALL + HALF * HEAD
    near, first_state = pl.pallas_call(
        project_body,
        out_shape=(shape((TP * NEAR_KV, 2 * TOKENS, 128), BF16), held((SEQS, HEAD, STATE), F32)),
        in_specs=[smem(), far_memory()] + [vmem()] * 8,
        out_specs=(vmem(),) * 2,
        scratch_shapes=[pltpu.VMEM((128, 128), F32), pltpu.VMEM((128, 128), F32), pltpu.SemaphoreType.DMA((SEQS,))],
    )(accepted, saved_states, hidden, input_gain, x_weight.T, z_weight.T, bc_weight.T, dt_weight.T, bc_rows, bc_kernel)
    first_state = near_memory(first_state)
    output_weight = near_memory(output_weight)
    arrived = near_memory(lax.all_to_all(near, NEAR, 0, 0, tiled=True))
    kept_pack, sent = pl.pallas_call(
        pack_body,
        out_shape=(held((pack_rows, 128), BF16), held((HEAD + 16, output_weight.shape[1]), BF16)),
        in_specs=[smem()] * 4 + [vmem()] * 5,
        out_specs=(vmem(),) * 2,
        cost_estimate=pl.CostEstimate(flops=4_000_000, bytes_accessed=3_000_000, transcendentals=0),
    )(
        accepted,
        dt_bias,
        decay_log,
        skip_scale,
        first_state,
        output_weight,
        x_rows,
        x_kernel,
        output_gain.reshape(1, HEAD),
    )
    got = lax.ppermute(sent, "c", [(0, 1), (1, 0)])
    far = pl.pallas_call(
        mix_body,
        out_shape=shape((lines, 128), BF16),
        in_specs=[vmem()] * 4,
        out_specs=vmem(),
        scratch_shapes=[pltpu.VMEM((TOKENS, 8), F32)],
    )(arrived, near_memory(kept_pack), near_memory(got), output_weight)
    landed = lax.all_to_all(far.reshape(KV_SIZE, LINES // 2, 2, 128), KV, 0, 0, tiled=True)
    landed = near_memory(landed.reshape(lines, 128))
    new_states, x_window, bc_window = pl.pallas_call(
        state_body,
        out_shape=(
            shape((SEQS, PROPS + 1, 1, HEAD, STATE), F32),
            shape((7, SEQS, HEAD), BF16),
            shape((7, SEQS, HEAD), BF16),
        ),
        in_specs=[smem()] * 3 + [vmem()] * 4,
        out_specs=(vmem(),) * 3,
        scratch_shapes=[pltpu.VMEM((TOKENS, 8), F32)],
        cost_estimate=pl.CostEstimate(flops=4_000_000, bytes_accessed=3_000_000, transcendentals=0),
    )(
        accepted,
        dt_bias,
        decay_log,
        arrived,
        first_state,
        x_kernel,
        x_rows,
    )
    mixed = pl.pallas_call(
        finish_body,
        out_shape=shape((TOKENS, TOKENS), BF16),
        in_specs=[vmem()],
        out_specs=vmem(),
        scratch_shapes=[pltpu.VMEM((8 * LINES, 128), F32), pltpu.VMEM((TOKENS, 128), F32)],
    )(landed)
    return (mixed, new_states, jnp.transpose(x_window, (1, 0, 2)), jnp.transpose(bc_window, (1, 0, 2)))


def solution(mesh):
    split = Mesh(mesh.devices.reshape(8, 4, 2, 2, mesh.shape["tp"]), ("z", "yh", "yl", "c", "tp"))
    return jax.shard_map(
        local,
        mesh=split,
        in_specs=(
            P(None, "tp"),
            P("tp"),
            P("tp", KV),
            P("tp", KV),
            P("tp", KV),
            P("tp", KV),
            P(None, KV),
            P(None, KV),
            P(KV),
            P(KV),
            P(KV),
            P(KV),
            P(KV, None),
            P("tp", None, KV, None, None),
            P("tp", None, KV),
            P("tp", None, KV),
            P("tp"),
        ),
        out_specs=(
            P("tp", KV),
            P("tp", None, KV, None, None),
            P("tp", None, KV),
            P("tp", None, KV),
        ),
        check_vma=False,
    )
```

time: 54 us -> 56.5 us (1.046)
  blocking collectives: 0 us -> 10.9 us
  waiting for transfers between devices: 19 us -> 11.4 us
  starting transfers between devices: 23.2 us -> 21.8 us
    all_to_all x0 -> x1, blocking collectives: none -> 10.9 us  [local(): arrived = near_memory(lax.all_to_all(near, NEAR, 0, 0, tiled=True))]
    all_to_all x1 -> x0, starting transfers between devices: 10.2 us -> none  [local(): arrived = near_memory(lax.all_to_all(near, NEAR, 0, 0, tiled=True))]
    ppermute x0 -> x1, starting transfers between devices: none -> 8.74 us  [local(): got = lax.ppermute(sent, 'c', [(0, 1), (1, 0)])]
    all_to_all x1 -> x0, waiting for transfers between devices: 3.96 us -> none  [local(): arrived = near_memory(lax.all_to_all(near, NEAR, 0, 0, tiled=True))]
    all_to_all x1, waiting for transfers between devices: 15 us -> 11.4 us  [local(): lax.all_to_all(far.reshape(KV_SIZE, LINES // 2, 2, 128), KV, 0, 0, tiled=...]
  transfers between devices with their start and end apart: 2 -> 2, of which waited for: 2 -> 1; matrix products, arithmetic and copies ran while one was open for 0% -> 0% of each run, Pallas kernels for 6% -> 5%
where the time goes in v3:
time: 56.5 us; the launch traced here: 56 us
  starting transfers between devices  21.8 us (39%)
  waiting for transfers between devices  11.4 us (20%)
  blocking collectives  10.9 us (19%)
  Pallas kernels  9.18 us (16%)
  between operations  2.67 us (5%)
    all_to_all x1, starting transfers between devices, local(): lax.all_to_all(far.reshape(KV_SIZE, LINES // 2, 2, 128), KV, 0, 0, tiled=...  13.1 us
    all_to_all x1, waiting for transfers between devices, local(): lax.all_to_all(far.reshape(KV_SIZE, LINES // 2, 2, 128), KV, 0, 0, tiled=...  11.4 us
    all_to_all x1, blocking collectives, local(): arrived = near_memory(lax.all_to_all(near, NEAR, 0, 0, tiled=True))  10.9 us
    ppermute x1, starting transfers between devices, local(): got = lax.ppermute(sent, 'c', [(0, 1), (1, 0)])  8.74 us
    pallas_call x1, Pallas kernels, local(): pl.pallas_call(project_body, out_shape=(shape((TP * NEAR_KV, 2 * TOKENS,...  3.17 us
    pallas_call x1, Pallas kernels, local(): pl.pallas_call(state_body, out_shape=(shape((SEQS, PROPS + 1, 1, HEAD, ST...  2.57 us
    pallas_call x1, Pallas kernels, local(): pl.pallas_call(mix_body, out_shape=shape((lines, 128), BF16), in_specs=[v...  1.82 us
  transfers between devices with their start and end apart: 2, of which 1 were waited for; matrix products, arithmetic and copies ran while one was open for 0% of the time, Pallas kernels for 5%

profile of v3, /device:TPU:1, one launch (start us, length us, event | category | flops | bytes accessed | tf_op | source)
XLA Modules:
  0.0 56.0 jit_solution(14786833227466471037)
XLA Ops:
  0.6 0.0 copy-start
  2.6 3.2 %shard_map.192 = (bf16[16,64,128]{2,1,0:T(8,128)(2,1)}, f32[8,64,128]{2,1,0:T(8,128)S(1)}) custom-call(s32[8]{0:T(128)} %accepted.5, f32[8,5,1,64,128]{4,3,2,1,0:T(8,128)} %saved.1, bf16[128,1024]{1,0:T(8,128)(2,1)} %hidden.1, bf16[1024]{0:T(1024)(128)(2,1)} %gain.1, bf16[64,1024]{1,0:T(8,128)(2,1)} %bitcast.13, bf16[64,1024]{1,0:T(8,128)(2,1)} %bitcast.14, ...), custom_call_target="tpu_custom_call" | custom-call | tf_op jit(solution)/shard_map/pallas_call | solution.py:433
  5.8 0.0 copy-done
  5.8 0.9 %shard_map.193 = (bf16[320,128]{1,0:T(8,128)(2,1)S(1)}, bf16[80,4096]{1,0:T(8,128)(2,1)S(1)}) custom-call(s32[8]{0:T(128)} %accepted.5, f32[1]{0:T(128)S(6)} %copy.21.dt_bias, f32[1]{0:T(128)S(6)} %copy.22.decay_log, f32[1]{0:T(128)S(6)} %copy.23.skip_scale, f32[8,64,128]{2,1,0:T(8,128)S(1)} %get-tuple-element.12.first_state, bf16[64,4096]{1,0:T(8,128)(2,1)S(1)} %copy-done, ...), custom_call_target="tpu_custom_call" | custom-call | flops 4000000 | bytes 3000000 | tf_op jit(solution)/shard_map/pallas_call | solution.py:443
  6.7 8.7 %collective-permute-start = (bf16[80,4096]{1,0:T(8,128)(2,1)S(1)}, bf16[80,4096]{1,0:T(8,128)(2,1)S(1)}, u32[]{:S(2)}, u32[]{:S(2)}) collective-permute-start(bf16[80,4096]{1,0:T(8,128)(2,1)S(1)} %get-tuple-element.14), channel_id=1, source_target_pairs={{0,4},{4,0},{1,5},{5,1},{2,6},{6,2},{3,7},{7,3},{8,12},{12,8},{9,1... | collective-permute-start | bytes 1966088 | tf_op jit(solution)/shard_map/ppermute | solution.py:460
  15.5 10.9 %all_to_all.10.arrived = bf16[16,64,128]{2,1,0:T(8,128)(2,1)S(1)} all-to-all(bf16[16,64,128]{2,1,0:T(8,128)(2,1)} %get-tuple-element.11), channel_id=1, replica_groups=mesh['z'=8,'yh'=4,'yl'=2,'c'=2,'tp'=4] {'yl','c','tp'}, dimensions={0} | all-to-all | bytes 524288 | tf_op jit(solution)/shard_map/all_to_all | solution.py:442
  26.3 0.0 collective-permute-done.got
  26.3 1.8 %shard_map.194 = bf16[768,128]{1,0:T(8,128)(2,1)} custom-call(bf16[16,64,128]{2,1,0:T(8,128)(2,1)S(1)} %all_to_all.10.arrived, bf16[320,128]{1,0:T(8,128)(2,1)S(1)} %get-tuple-element.13.kept_pack, bf16[80,4096]{1,0:T(8,128)(2,1)S(1)} %collective-permute-done.got, bf16[64,4096]{1,0:T(8,128)(2,1)S(1)} %copy-done), custom_call_target="tpu_custom_call" | custom-call | tf_op jit(solution)/shard_map/pallas_call | solution.py:461
  28.2 13.1 %all-to-all-start.1 = ((bf16[128,3,2,128]{3,2,1,0:T(2,128)(2,1)}), bf16[128,3,2,128]{3,2,1,0:T(2,128)(2,1)S(1)}, u32[]{:S(2)}, u32[]{:S(2)}) async-start(bf16[128,3,2,128]{3,2,1,0:T(2,128)(2,1)} %bitcast.12), calls=%async_computation.1 | async-start | bytes 393216 | tf_op jit(solution)/shard_map/all_to_all | solution.py:468
  41.3 2.6 %shard_map.196 = (f32[8,5,1,64,128]{4,3,2,1,0:T(8,128)}, bf16[7,8,64]{2,1,0:T(8,128)(2,1)}, bf16[7,8,64]{2,1,0:T(8,128)(2,1)}) custom-call(s32[8]{0:T(128)} %accepted.5, f32[1]{0:T(128)S(6)} %copy.21.dt_bias, f32[1]{0:T(128)S(6)} %copy.22.decay_log, bf16[16,64,128]{2,1,0:T(8,128)(2,1)S(1)} %all_to_all.10.arrived, ...), custom_call_target="tpu_custom_call" | custom-call | flops 4000000 | bytes 3000000 | tf_op jit(solution)/shard_map/pallas_call | solution.py:470
  43.8 11.4 %all-to-all-done.1 = bf16[128,3,2,128]{3,2,1,0:T(2,128)(2,1)S(1)} async-done(((bf16[128,3,2,128]{3,2,1,0:T(2,128)(2,1)}), bf16[128,3,2,128]{3,2,1,0:T(2,128)(2,1)S(1)}, u32[]{:S(2)}, u32[]{:S(2)}) %all-to-all-start.1) | async-done | bytes 196640 | tf_op jit(solution)/shard_map/all_to_all | solution.py:468
  55.2 0.7 %shard_map.195 = bf16[32,32]{1,0:T(8,128)(2,1)} custom-call(bf16[768,128]{1,0:T(8,128)(2,1)S(1)} %bitcast.11), custom_call_target="tpu_custom_call" | custom-call | tf_op jit(solution)/shard_map/pallas_call | solution.py:490
Async XLA Ops:
  0.6 5.2 %copy-start = (bf16[64,4096]{1,0:T(8,128)(2,1)S(1)}, bf16[64,4096]{1,0:T(8,128)(2,1)}, u32[]{:S(2)}) copy-start(bf16[64,4096]{1,0:T(8,128)(2,1)} %weight.3) | copy-start | bytes 1572868
  6.7 19.6 %collective-permute-start = (bf16[80,4096]{1,0:T(8,128)(2,1)S(1)}, bf16[80,4096]{1,0:T(8,128)(2,1)S(1)}, u32[]{:S(2)}, u32[]{:S(2)}) collective-permute-start(bf16[80,4096]{1,0:T(8,128)(2,1)S(1)} %get-tuple-element.14), channel_id=1, source_target_pairs={{0,4},{4,0},{1,5},{5,1},{2,6},{6,2},{3,7},{7,3},{8,12},{12,8},{9,1... | collective-permute-start | bytes 1966088 | tf_op jit(solution)/shard_map/ppermute | solution.py:460
  28.2 27.1 %all-to-all-start.1 = ((bf16[128,3,2,128]{3,2,1,0:T(2,128)(2,1)}), bf16[128,3,2,128]{3,2,1,0:T(2,128)(2,1)S(1)}, u32[]{:S(2)}, u32[]{:S(2)}) async-start(bf16[128,3,2,128]{3,2,1,0:T(2,128)(2,1)} %bitcast.12), calls=%async_computation.1 | async-start | bytes 393216 | tf_op jit(solution)/shard_map/all_to_all | solution.py:468

commit v4 on v3

--- a/solution.py
+++ b/solution.py
@@ -70,16 +70,15 @@
 
 
 def kept_rows(history, accepted):
-    rows = rows_of((SEQS, HEAD))
-    column = jnp.zeros((SEQS, HEAD), jnp.int32)
-    for s in range(SEQS):
-        column = jnp.where(rows == s, accepted[s], column)
+    line = jnp.broadcast_to(accepted[...].astype(F32)[None, :], (SEQS, SEQS))
+    own = lanes_of((SEQS, SEQS)) == rows_of((SEQS, SEQS))
+    column = jnp.sum(jnp.where(own, line, 0.0), axis=1, keepdims=True)
     whole = [history[i].astype(F32) for i in range(7)]
     kept = []
     for m in range(3):
         row = whole[m]
         for a in range(1, PROPS + 1):
-            row = jnp.where(column == a, whole[m + a], row)
+            row = jnp.where(column == float(a), whole[m + a], row)
         kept.append(row)
     return kept
 
@@ -104,27 +103,59 @@
 
 
 def project_body(
+    accepted_far,
+    saved,
+    hidden_far,
+    x_weight_far,
+    z_weight_far,
+    bc_weight_far,
+    gain_far,
+    dt_weight_far,
+    bc_history_far,
+    bc_kernel_far,
+    message,
+    first_state,
+    chosen,
     accepted,
-    saved,
     hidden,
-    gain,
     x_weight,
     z_weight,
     bc_weight,
+    gain,
     dt_weight,
     bc_history,
     bc_kernel,
-    message,
-    first_state,
     first,
     second,
-    arrivals,
+    blocks,
+    coming,
+    reading,
+    leaving,
 ):
-    copies = [
-        pltpu.make_async_copy(saved.at[s, accepted[s], 0], first_state.at[s], arrivals.at[s]) for s in range(SEQS)
+    sources = [
+        accepted_far,
+        hidden_far,
+        x_weight_far,
+        z_weight_far,
+        bc_weight_far,
+        gain_far,
+        dt_weight_far,
+        bc_history_far,
+        bc_kernel_far,
+        accepted_far,
     ]
-    for copy in copies:
+    targets = [chosen, hidden, x_weight, z_weight, bc_weight, gain, dt_weight, bc_history, bc_kernel, accepted]
+    inputs = [pltpu.make_async_copy(a, b, coming.at[i]) for i, (a, b) in enumerate(zip(sources, targets))]
+    for copy in inputs:
         copy.start()
+    inputs[0].wait()
+    reads = [
+        pltpu.make_async_copy(saved.at[s, chosen[s], 0], first_state.at[s], reading.at[s]) for s in range(SEQS)
+    ]
+    for copy in reads:
+        copy.start()
+    for copy in inputs[1:]:
+        copy.wait()
     wide = hidden[...].astype(F32)
     scaled = (wide * gain[...].astype(F32)[None, :]).astype(BF16)
     squares = jnp.sum(wide * wide, axis=1, keepdims=True)
@@ -143,23 +174,25 @@
     extra = [jnp.concatenate([empty, row], axis=1) for row in kept_rows(bc_history, accepted)]
     taps = jnp.concatenate([bc_kernel[...].astype(F32), jnp.zeros((4, HEAD), F32)], axis=0)
     taps = jnp.concatenate([empty, taps], axis=1)
+    copies = []
     for j in range(TP):
         top = [first[pl.ds(TOKENS * j + t, SEQS, stride=PROPS), :] for t in range(PROPS)]
         low = [second[pl.ds(TOKENS * j + t, SEQS, stride=PROPS), :] for t in range(PROPS)]
         ending = jnp.where(rows < 4, taps, pltpu.roll(lines, (64 - 32 * j) % 128, 1))
         low = [jnp.where(upper, e, v) for e, v in zip([*extra, ending], low)]
-        block = jnp.concatenate(top + low, axis=0).astype(BF16)
+        blocks[j] = jnp.concatenate(top + low, axis=0).astype(BF16)
         for g in range(NEAR_KV):
-            message[g * TP + j] = block
-    for copy in copies:
+            copies.append(pltpu.make_async_copy(blocks.at[j], message.at[g * TP + j], leaving.at[g * TP + j]))
+            copies[-1].start()
+    for copy in reads + copies:
         copy.wait()
 
 
 def pack_body(
-    accepted,
     dt_bias,
     decay_log,
     skip_scale,
+    accepted,
     first_state,
     weight,
     x_history,
@@ -179,12 +212,16 @@
     small = [small[0] + gain_row] + [a + b for a, b in zip(small[1:4], terms)] + small[4:]
     small.append(jnp.zeros(TILE, F32))
     kept_pack[0:SMALL, :] = jnp.concatenate([jnp.where(rows < HALF, tile, 0.0) for tile in small], axis=0).astype(BF16)
-    kept_pack[SMALL:, :] = first_state[pl.ds(HALF * core, HALF)].reshape(HALF * HEAD, STATE).astype(BF16)
+    for i in range(HALF):
+        own = HALF * core + i
+        kept_pack[SMALL + HEAD * i : SMALL + HEAD * (i + 1), :] = first_state[own].astype(BF16)
     sent[0:HEAD, :] = weight[...]
     small = [jnp.where(rows < HALF, 0.0, tile) for tile in small]
-    states = first_state[pl.ds(HALF - HALF * core, HALF)].reshape(HALF * HEAD, STATE)
     blocks = [jnp.concatenate(small[2 * i : 2 * i + 2], axis=0) for i in range(SMALL // 16)]
-    blocks += [states[16 * i : 16 * i + 16] for i in range(HALF * HEAD // 16)]
+    for i in range(HALF):
+        other = HALF - HALF * core + i
+        state = first_state[other]
+        blocks += [state[16 * k : 16 * k + 16] for k in range(HEAD // 16)]
     blocks += [jnp.zeros((16, 128), F32)] * (weight.shape[1] // 128 - len(blocks))
     for i, block in enumerate(blocks):
         sent[HEAD : HEAD + 16, 128 * i : 128 * i + 128] = block.astype(BF16)
@@ -201,7 +238,7 @@
     return lax.rsqrt((ending[5:6] + ending[6:7]) / D + EPSILON)
 
 
-def mix_body(arrived, kept_pack, got, weight, message, columns):
+def mix_body(arrived, kept_pack, got, weight, message, columns, block_rows, leaving):
     core = lax.axis_index("c")
     pair = lax.axis_index("yl") * 2
     mine = lax.axis_index("tp")
@@ -285,6 +322,7 @@
     square_line = jnp.sum(spot, axis=0, keepdims=True)
     high = rounded(square_line)
     lines = jnp.where(rows % 2 == 0, high, square_line - high)
+    copies = []
     for i in range(weight.shape[1] // 256):
         cut = slice(256 * i, 256 * (i + 1))
         both_weights = jnp.concatenate([weight[:, cut], got[0:HEAD, cut]], axis=0)
@@ -305,13 +343,19 @@
                 jnp.where(rows < 2, spots[1], jnp.where(rows < 4, lines, spots[2])),
                 jnp.where((rows >= 2) & (rows < 6), spots[3], lines),
             ]
-        message[48 * i : 48 * (i + 1), :] = jnp.concatenate(pieces, axis=0).astype(BF16)
+        block_rows[48 * i : 48 * (i + 1), :] = jnp.concatenate(pieces, axis=0).astype(BF16)
+        if i % 4 == 3:
+            part = pl.ds(48 * (i - 3), 192)
+            copies.append(pltpu.make_async_copy(block_rows.at[part], message.at[part], leaving.at[i // 4]))
+            copies[-1].start()
+    for copy in copies:
+        copy.wait()
 
 
 def state_body(
-    accepted,
     dt_bias,
     decay_log,
+    accepted,
     arrived,
     first_state,
     x_kernel,
@@ -433,37 +477,54 @@
     near, first_state = pl.pallas_call(
         project_body,
         out_shape=(shape((TP * NEAR_KV, 2 * TOKENS, 128), BF16), held((SEQS, HEAD, STATE), F32)),
-        in_specs=[smem(), far_memory()] + [vmem()] * 8,
-        out_specs=(vmem(),) * 2,
-        scratch_shapes=[pltpu.VMEM((128, 128), F32), pltpu.VMEM((128, 128), F32), pltpu.SemaphoreType.DMA((SEQS,))],
-    )(accepted, saved_states, hidden, input_gain, x_weight.T, z_weight.T, bc_weight.T, dt_weight.T, bc_rows, bc_kernel)
+        in_specs=[far_memory()] * 10,
+        out_specs=(far_memory(), vmem()),
+        scratch_shapes=[
+            pltpu.SMEM(accepted.shape, jnp.int32),
+            pltpu.VMEM(accepted.shape, jnp.int32),
+            pltpu.VMEM(hidden.shape, BF16),
+            pltpu.VMEM(x_weight.T.shape, BF16),
+            pltpu.VMEM(z_weight.T.shape, BF16),
+            pltpu.VMEM(bc_weight.T.shape, BF16),
+            pltpu.VMEM(input_gain.shape, BF16),
+            pltpu.VMEM(dt_weight.T.shape, BF16),
+            pltpu.VMEM(bc_rows.shape, BF16),
+            pltpu.VMEM(bc_kernel.shape, BF16),
+            pltpu.VMEM((128, 128), F32),
+            pltpu.VMEM((128, 128), F32),
+            pltpu.VMEM((TP, 2 * TOKENS, 128), BF16),
+            pltpu.SemaphoreType.DMA((10,)),
+            pltpu.SemaphoreType.DMA((SEQS,)),
+            pltpu.SemaphoreType.DMA((TP * NEAR_KV,)),
+        ],
+    )(accepted, saved_states, hidden, x_weight.T, z_weight.T, bc_weight.T, input_gain, dt_weight.T, bc_rows, bc_kernel)
     first_state = near_memory(first_state)
     output_weight = near_memory(output_weight)
     arrived = near_memory(lax.all_to_all(near, NEAR, 0, 0, tiled=True))
     kept_pack, sent = pl.pallas_call(
         pack_body,
         out_shape=(held((pack_rows, 128), BF16), held((HEAD + 16, output_weight.shape[1]), BF16)),
-        in_specs=[smem()] * 4 + [vmem()] * 5,
+        in_specs=[smem()] * 3 + [vmem()] * 6,
         out_specs=(vmem(),) * 2,
         cost_estimate=pl.CostEstimate(flops=4_000_000, bytes_accessed=3_000_000, transcendentals=0),
     )(
-        accepted,
         dt_bias,
         decay_log,
         skip_scale,
+        near_memory(accepted),
         first_state,
         output_weight,
-        x_rows,
-        x_kernel,
-        output_gain.reshape(1, HEAD),
+        near_memory(x_rows),
+        near_memory(x_kernel),
+        near_memory(output_gain.reshape(1, HEAD)),
     )
     got = lax.ppermute(sent, "c", [(0, 1), (1, 0)])
     far = pl.pallas_call(
         mix_body,
         out_shape=shape((lines, 128), BF16),
         in_specs=[vmem()] * 4,
-        out_specs=vmem(),
-        scratch_shapes=[pltpu.VMEM((TOKENS, 8), F32)],
+        out_specs=far_memory(),
+        scratch_shapes=[pltpu.VMEM((TOKENS, 8), F32), pltpu.VMEM((lines, 128), BF16), pltpu.SemaphoreType.DMA((4,))],
     )(arrived, near_memory(kept_pack), near_memory(got), output_weight)
     landed = lax.all_to_all(far.reshape(KV_SIZE, LINES // 2, 2, 128), KV, 0, 0, tiled=True)
     landed = near_memory(landed.reshape(lines, 128))
@@ -474,14 +535,14 @@
             shape((7, SEQS, HEAD), BF16),
             shape((7, SEQS, HEAD), BF16),
         ),
-        in_specs=[smem()] * 3 + [vmem()] * 4,
+        in_specs=[smem()] * 2 + [vmem()] * 5,
         out_specs=(vmem(),) * 3,
         scratch_shapes=[pltpu.VMEM((TOKENS, 8), F32)],
         cost_estimate=pl.CostEstimate(flops=4_000_000, bytes_accessed=3_000_000, transcendentals=0),
     )(
-        accepted,
         dt_bias,
         decay_log,
+        accepted,
         arrived,
         first_state,
         x_kernel,

time: 56.5 us -> 55.1 us (0.975)
  Pallas kernels: 9.18 us -> 7.81 us
    pallas_call x1, Pallas kernels: 0.88 us -> 0.09 us  [local(): pl.pallas_call(pack_body, out_shape=(held((pack_rows, 128), BF16), held((...]
    pallas_call x1, Pallas kernels: 3.17 us -> 2.55 us  [local(): pl.pallas_call(project_body, out_shape=(shape((TP * NEAR_KV, 2 * TOKENS,...]
where the time goes in v4:
time: 55.1 us; the launch traced here: 54.6 us
  starting transfers between devices  21.8 us (40%)
  waiting for transfers between devices  11.3 us (21%)
  blocking collectives  10.9 us (20%)
  Pallas kernels  7.81 us (14%)
  between operations  2.74 us (5%)
    all_to_all x1, starting transfers between devices, local(): lax.all_to_all(far.reshape(KV_SIZE, LINES // 2, 2, 128), KV, 0, 0, tiled=...  13.1 us
    all_to_all x1, waiting for transfers between devices, local(): lax.all_to_all(far.reshape(KV_SIZE, LINES // 2, 2, 128), KV, 0, 0, tiled=...  11.3 us
    all_to_all x1, blocking collectives, local(): arrived = near_memory(lax.all_to_all(near, NEAR, 0, 0, tiled=True))  10.9 us
    ppermute x1, starting transfers between devices, local(): got = lax.ppermute(sent, 'c', [(0, 1), (1, 0)])  8.74 us
    pallas_call x1, Pallas kernels, local(): pl.pallas_call(state_body, out_shape=(shape((SEQS, PROPS + 1, 1, HEAD, ST...  2.62 us
    pallas_call x1, Pallas kernels, local(): pl.pallas_call(project_body, out_shape=(shape((TP * NEAR_KV, 2 * TOKENS,...  2.55 us
    pallas_call x1, Pallas kernels, local(): pl.pallas_call(mix_body, out_shape=shape((lines, 128), BF16), in_specs=[v...  1.8 us
  transfers between devices with their start and end apart: 2, of which 1 were waited for; matrix products, arithmetic and copies ran while one was open for 0% of the time, Pallas kernels for 5%

profile of v4, /device:TPU:1, one launch (start us, length us, event | category | flops | bytes accessed | tf_op | source)
XLA Modules:
  0.0 54.6 jit_solution(5986592065448254926)
XLA Ops:
  0.6 0.0 copy-start.2
  0.6 0.0 copy-start
  0.7 0.0 copy-start.3
  0.7 0.0 copy-start.1
  0.7 0.0 copy-start.4
  2.7 2.6 %shard_map.192 = (bf16[16,64,128]{2,1,0:T(8,128)(2,1)}, f32[8,64,128]{2,1,0:T(8,128)S(1)}) custom-call(s32[8]{0:T(128)} %accepted.3, f32[8,5,1,64,128]{4,3,2,1,0:T(8,128)} %saved.1, bf16[128,1024]{1,0:T(8,128)(2,1)} %hidden_far.1, bf16[64,1024]{1,0:T(8,128)(2,1)} %bitcast.16, bf16[64,1024]{1,0:T(8,128)(2,1)} %bitcast.17, bf16[64,1024]{1,0:T(8,128)(2,1)} %bitcast.18, ...), custom_call_target="tpu_custom_call" | custom-call | tf_op jit(solution)/shard_map/pallas_call | solution.py:477
  5.2 0.0 copy-done.2
  5.3 0.0 copy-done
  5.3 0.0 copy-done.3
  5.3 0.0 copy-done.1
  5.3 0.0 copy-done.4
  5.3 0.1 shard_map.193
  5.4 8.7 %collective-permute-start = (bf16[80,4096]{1,0:T(8,128)(2,1)S(1)}, bf16[80,4096]{1,0:T(8,128)(2,1)S(1)}, u32[]{:S(2)}, u32[]{:S(2)}) collective-permute-start(bf16[80,4096]{1,0:T(8,128)(2,1)S(1)} %get-tuple-element.14), channel_id=1, source_target_pairs={{0,4},{4,0},{1,5},{5,1},{2,6},{6,2},{3,7},{7,3},{8,12},{12,8},{9,1... | collective-permute-start | bytes 1966088 | tf_op jit(solution)/shard_map/ppermute | solution.py:521
  14.1 10.9 %all_to_all.10.arrived = bf16[16,64,128]{2,1,0:T(8,128)(2,1)S(1)} all-to-all(bf16[16,64,128]{2,1,0:T(8,128)(2,1)} %get-tuple-element.11), channel_id=1, replica_groups=mesh['z'=8,'yh'=4,'yl'=2,'c'=2,'tp'=4] {'yl','c','tp'}, dimensions={0} | all-to-all | bytes 524288 | tf_op jit(solution)/shard_map/all_to_all | solution.py:503
  25.0 0.0 collective-permute-done.got
  25.0 1.8 %shard_map.194 = bf16[768,128]{1,0:T(8,128)(2,1)} custom-call(bf16[16,64,128]{2,1,0:T(8,128)(2,1)S(1)} %all_to_all.10.arrived, bf16[320,128]{1,0:T(8,128)(2,1)S(1)} %get-tuple-element.13.kept_pack, bf16[80,4096]{1,0:T(8,128)(2,1)S(1)} %collective-permute-done.got, bf16[64,4096]{1,0:T(8,128)(2,1)S(1)} %copy-done), custom_call_target="tpu_custom_call" | custom-call | tf_op jit(solution)/shard_map/pallas_call | solution.py:522
  26.8 13.1 %all-to-all-start.1 = ((bf16[128,3,2,128]{3,2,1,0:T(2,128)(2,1)}), bf16[128,3,2,128]{3,2,1,0:T(2,128)(2,1)S(1)}, u32[]{:S(2)}, u32[]{:S(2)}) async-start(bf16[128,3,2,128]{3,2,1,0:T(2,128)(2,1)} %bitcast.15), calls=%async_computation.1 | async-start | bytes 393216 | tf_op jit(solution)/shard_map/all_to_all | solution.py:529
  39.9 2.6 %shard_map.196 = (f32[8,5,1,64,128]{4,3,2,1,0:T(8,128)}, bf16[7,8,64]{2,1,0:T(8,128)(2,1)}, bf16[7,8,64]{2,1,0:T(8,128)(2,1)}) custom-call(f32[1]{0:T(128)S(6)} %copy.21.dt_bias, f32[1]{0:T(128)S(6)} %copy.22.decay_log, s32[8]{0:T(128)} %accepted.3, bf16[16,64,128]{2,1,0:T(8,128)(2,1)S(1)} %all_to_all.10.arrived, ...), custom_call_target="tpu_custom_call" | custom-call | flops 4000000 | bytes 3000000 | tf_op jit(solution)/shard_map/pallas_call | solution.py:531
  42.6 11.3 %all-to-all-done.1 = bf16[128,3,2,128]{3,2,1,0:T(2,128)(2,1)S(1)} async-done(((bf16[128,3,2,128]{3,2,1,0:T(2,128)(2,1)}), bf16[128,3,2,128]{3,2,1,0:T(2,128)(2,1)S(1)}, u32[]{:S(2)}, u32[]{:S(2)}) %all-to-all-start.1) | async-done | bytes 196640 | tf_op jit(solution)/shard_map/all_to_all | solution.py:529
  53.9 0.7 %shard_map.195 = bf16[32,32]{1,0:T(8,128)(2,1)} custom-call(bf16[768,128]{1,0:T(8,128)(2,1)S(1)} %bitcast.11), custom_call_target="tpu_custom_call" | custom-call | tf_op jit(solution)/shard_map/pallas_call | solution.py:551
Async XLA Ops:
  0.6 4.6 %copy-start.2 = (s32[8]{0:T(128)S(1)}, s32[8]{0:T(128)}, u32[]{:S(2)}) copy-start(s32[8]{0:T(128)} %accepted.3) | copy-start | bytes 100
  0.6 4.6 %copy-start = (bf16[64,4096]{1,0:T(8,128)(2,1)S(1)}, bf16[64,4096]{1,0:T(8,128)(2,1)}, u32[]{:S(2)}) copy-start(bf16[64,4096]{1,0:T(8,128)(2,1)} %weight.3) | copy-start | bytes 1572868
  0.7 4.6 %copy-start.3 = (bf16[4,64]{1,0:T(4,128)(2,1)S(1)}, bf16[4,64]{1,0:T(4,128)(2,1)}, u32[]{:S(2)}) copy-start(bf16[4,64]{1,0:T(4,128)(2,1)} %x_kernel.3) | copy-start | bytes 1540
  0.7 4.6 %copy-start.1 = (bf16[8,7,64]{2,0,1:T(8,128)(2,1)S(1)}, bf16[8,7,64]{2,0,1:T(8,128)(2,1)}, u32[]{:S(2)}) copy-start(bf16[8,7,64]{2,0,1:T(8,128)(2,1)} %param.31) | copy-start | bytes 21508
  0.7 4.6 %copy-start.4 = (bf16[64]{0:T(256)(128)(2,1)S(1)}, bf16[64]{0:T(256)(128)(2,1)}, u32[]{:S(2)}) copy-start(bf16[64]{0:T(256)(128)(2,1)} %param.28) | copy-start | bytes 388
  5.4 19.6 %collective-permute-start = (bf16[80,4096]{1,0:T(8,128)(2,1)S(1)}, bf16[80,4096]{1,0:T(8,128)(2,1)S(1)}, u32[]{:S(2)}, u32[]{:S(2)}) collective-permute-start(bf16[80,4096]{1,0:T(8,128)(2,1)S(1)} %get-tuple-element.14), channel_id=1, source_target_pairs={{0,4},{4,0},{1,5},{5,1},{2,6},{6,2},{3,7},{7,3},{8,12},{12,8},{9,1... | collective-permute-start | bytes 1966088 | tf_op jit(solution)/shard_map/ppermute | solution.py:521
  26.8 27.1 %all-to-all-start.1 = ((bf16[128,3,2,128]{3,2,1,0:T(2,128)(2,1)}), bf16[128,3,2,128]{3,2,1,0:T(2,128)(2,1)S(1)}, u32[]{:S(2)}, u32[]{:S(2)}) async-start(bf16[128,3,2,128]{3,2,1,0:T(2,128)(2,1)} %bitcast.15), calls=%async_computation.1 | async-start | bytes 393216 | tf_op jit(solution)/shard_map/all_to_all | solution.py:529

commit v5 on v4

--- a/solution.py
+++ b/solution.py
@@ -23,6 +23,8 @@
 STATE = 128
 LINES = 6
 TILE = (8, 128)
+FAR_FIRST = 88
+NEAR_FIRST = 0
 SMALL = 64
 
 F32 = jnp.float32
@@ -182,7 +184,7 @@
         low = [jnp.where(upper, e, v) for e, v in zip([*extra, ending], low)]
         blocks[j] = jnp.concatenate(top + low, axis=0).astype(BF16)
         for g in range(NEAR_KV):
-            copies.append(pltpu.make_async_copy(blocks.at[j], message.at[g * TP + j], leaving.at[g * TP + j]))
+            copies.append(pltpu.make_async_copy(blocks.at[j], message.at[g * TP + (j - NEAR_FIRST) % TP], leaving.at[g * TP + j]))
             copies[-1].start()
     for copy in reads + copies:
         copy.wait()
@@ -241,7 +243,7 @@
 def mix_body(arrived, kept_pack, got, weight, message, columns, block_rows, leaving):
     core = lax.axis_index("c")
     pair = lax.axis_index("yl") * 2
-    mine = lax.axis_index("tp")
+    mine = (lax.axis_index("tp") + TP - NEAR_FIRST) % TP
     lanes = lanes_of(TILE)
     rows = rows_of(TILE)
     lower = lanes < HEAD
@@ -323,8 +325,10 @@
     high = rounded(square_line)
     lines = jnp.where(rows % 2 == 0, high, square_line - high)
     copies = []
-    for i in range(weight.shape[1] // 256):
-        cut = slice(256 * i, 256 * (i + 1))
+    chunks = weight.shape[1] // 256
+    for i in range(chunks):
+        spot = (i + FAR_FIRST // 8) % chunks
+        cut = slice(256 * spot, 256 * (spot + 1))
         both_weights = jnp.concatenate([weight[:, cut], got[0:HEAD, cut]], axis=0)
         product = jnp.dot(turns, both_weights, preferred_element_type=F32)
         pieces = []
@@ -366,7 +370,7 @@
     columns,
 ):
     place = lax.axis_index(("yl", "c"))
-    mine = lax.axis_index("tp")
+    mine = (lax.axis_index("tp") + TP - NEAR_FIRST) % TP
     lanes = lanes_of(TILE)
     lower = lanes < HEAD
     own = summed_over_tp(arrived, place, 0)
@@ -500,7 +504,8 @@
     )(accepted, saved_states, hidden, x_weight.T, z_weight.T, bc_weight.T, input_gain, dt_weight.T, bc_rows, bc_kernel)
     first_state = near_memory(first_state)
     output_weight = near_memory(output_weight)
-    arrived = near_memory(lax.all_to_all(near, NEAR, 0, 0, tiled=True))
+    order = [[g * TP + (k + NEAR_FIRST) % TP for g in range(NEAR_KV) for k in range(TP)]]
+    arrived = near_memory(lax.all_to_all(near, NEAR, 0, 0, tiled=True, axis_index_groups=order))
     kept_pack, sent = pl.pallas_call(
         pack_body,
         out_shape=(held((pack_rows, 128), BF16), held((HEAD + 16, output_weight.shape[1]), BF16)),
@@ -526,7 +531,9 @@
         out_specs=far_memory(),
         scratch_shapes=[pltpu.VMEM((TOKENS, 8), F32), pltpu.VMEM((lines, 128), BF16), pltpu.SemaphoreType.DMA((4,))],
     )(arrived, near_memory(kept_pack), near_memory(got), output_weight)
-    landed = lax.all_to_all(far.reshape(KV_SIZE, LINES // 2, 2, 128), KV, 0, 0, tiled=True)
+    order = [[(i + FAR_FIRST) % KV_SIZE for i in range(KV_SIZE)]]
+    far = far.reshape(KV_SIZE, LINES // 2, 2, 128)
+    landed = lax.all_to_all(far, KV, 0, 0, tiled=True, axis_index_groups=order)
     landed = near_memory(landed.reshape(lines, 128))
     new_states, x_window, bc_window = pl.pallas_call(
         state_body,

time: 55.1 us -> 50.1 us (0.909)
  waiting for transfers between devices: 11.3 us -> 3.56 us
  starting transfers between devices: 21.8 us -> 24.7 us
    all_to_all x1, waiting for transfers between devices: 11.3 us -> 3.56 us  [local(): landed = lax.all_to_all(far, KV, 0, 0, tiled=True, axis_index_groups=order)]
    all_to_all x1, starting transfers between devices: 13.1 us -> 15.9 us  [local(): landed = lax.all_to_all(far, KV, 0, 0, tiled=True, axis_index_groups=order)]
where the time goes in v5:
time: 50.1 us; the launch traced here: 49.7 us
  starting transfers between devices  24.7 us (49%)
  blocking collectives  10.9 us (22%)
  Pallas kernels  7.81 us (16%)
  waiting for transfers between devices  3.56 us (7%)
  between operations  2.74 us (5%)
    all_to_all x1, starting transfers between devices, local(): landed = lax.all_to_all(far, KV, 0, 0, tiled=True, axis_index_groups=order)  15.9 us
    all_to_all x1, blocking collectives, local(): lax.all_to_all(near, NEAR, 0, 0, tiled=True, axis_index_groups=order)  10.9 us
    ppermute x1, starting transfers between devices, local(): got = lax.ppermute(sent, 'c', [(0, 1), (1, 0)])  8.74 us
    all_to_all x1, waiting for transfers between devices, local(): landed = lax.all_to_all(far, KV, 0, 0, tiled=True, axis_index_groups=order)  3.56 us
    pallas_call x1, Pallas kernels, local(): pl.pallas_call(state_body, out_shape=(shape((SEQS, PROPS + 1, 1, HEAD, ST...  2.62 us
    pallas_call x1, Pallas kernels, local(): pl.pallas_call(project_body, out_shape=(shape((TP * NEAR_KV, 2 * TOKENS,...  2.55 us
    pallas_call x1, Pallas kernels, local(): pl.pallas_call(mix_body, out_shape=shape((lines, 128), BF16), in_specs=[v...  1.8 us
  transfers between devices with their start and end apart: 2, of which 1 were waited for; matrix products, arithmetic and copies ran while one was open for 0% of the time, Pallas kernels for 5%

profile of v5, /device:TPU:1, one launch (start us, length us, event | category | flops | bytes accessed | tf_op | source)
XLA Modules:
  0.0 49.7 jit_solution(5415012118990463544)
XLA Ops:
  0.6 0.0 copy-start.2
  0.6 0.0 copy-start
  0.7 0.0 copy-start.3
  0.7 0.0 copy-start.1
  0.7 0.0 copy-start.4
  2.7 2.6 %shard_map.192 = (bf16[16,64,128]{2,1,0:T(8,128)(2,1)}, f32[8,64,128]{2,1,0:T(8,128)S(1)}) custom-call(s32[8]{0:T(128)} %accepted.3, f32[8,5,1,64,128]{4,3,2,1,0:T(8,128)} %saved.1, bf16[128,1024]{1,0:T(8,128)(2,1)} %hidden_far.1, bf16[64,1024]{1,0:T(8,128)(2,1)} %bitcast.16, bf16[64,1024]{1,0:T(8,128)(2,1)} %bitcast.17, bf16[64,1024]{1,0:T(8,128)(2,1)} %bitcast.18, ...), custom_call_target="tpu_custom_call" | custom-call | tf_op jit(solution)/shard_map/pallas_call | solution.py:481
  5.2 0.0 copy-done.2
  5.3 0.0 copy-done
  5.3 0.0 copy-done.3
  5.3 0.0 copy-done.1
  5.3 0.0 copy-done.4
  5.3 0.1 shard_map.193
  5.4 8.7 %collective-permute-start = (bf16[80,4096]{1,0:T(8,128)(2,1)S(1)}, bf16[80,4096]{1,0:T(8,128)(2,1)S(1)}, u32[]{:S(2)}, u32[]{:S(2)}) collective-permute-start(bf16[80,4096]{1,0:T(8,128)(2,1)S(1)} %get-tuple-element.14), channel_id=1, source_target_pairs={{0,4},{4,0},{1,5},{5,1},{2,6},{6,2},{3,7},{7,3},{8,12},{12,8},{9,1... | collective-permute-start | bytes 1966088 | tf_op jit(solution)/shard_map/ppermute | solution.py:526
  14.1 10.9 %all_to_all.10.arrived = bf16[16,64,128]{2,1,0:T(8,128)(2,1)S(1)} all-to-all(bf16[16,64,128]{2,1,0:T(8,128)(2,1)} %get-tuple-element.11), channel_id=1, replica_groups={{0,1,2,3,4,5,6,7,8,9,10,11,12,13,14,15},{16,17,18,19,20,21,22,23,24,25,..., dimensions={0} | all-to-all | bytes 524288 | tf_op jit(solution)/shard_map/all_to_all | solution.py:508
  25.0 0.0 collective-permute-done.got
  25.0 1.8 %shard_map.194 = bf16[768,128]{1,0:T(8,128)(2,1)} custom-call(bf16[16,64,128]{2,1,0:T(8,128)(2,1)S(1)} %all_to_all.10.arrived, bf16[320,128]{1,0:T(8,128)(2,1)S(1)} %get-tuple-element.13.kept_pack, bf16[80,4096]{1,0:T(8,128)(2,1)S(1)} %collective-permute-done.got, bf16[64,4096]{1,0:T(8,128)(2,1)S(1)} %copy-done), custom_call_target="tpu_custom_call" | custom-call | tf_op jit(solution)/shard_map/pallas_call | solution.py:527
  26.8 15.9 %all-to-all-start.1 = ((bf16[128,3,2,128]{3,2,1,0:T(2,128)(2,1)}), bf16[128,3,2,128]{3,2,1,0:T(2,128)(2,1)S(1)}, u32[]{:S(2)}, u32[]{:S(2)}) async-start(bf16[128,3,2,128]{3,2,1,0:T(2,128)(2,1)} %bitcast.15), calls=%async_computation.1 | async-start | bytes 393216 | tf_op jit(solution)/shard_map/all_to_all | solution.py:536
  42.7 2.6 %shard_map.196 = (f32[8,5,1,64,128]{4,3,2,1,0:T(8,128)}, bf16[7,8,64]{2,1,0:T(8,128)(2,1)}, bf16[7,8,64]{2,1,0:T(8,128)(2,1)}) custom-call(f32[1]{0:T(128)S(6)} %copy.21.dt_bias, f32[1]{0:T(128)S(6)} %copy.22.decay_log, s32[8]{0:T(128)} %accepted.3, bf16[16,64,128]{2,1,0:T(8,128)(2,1)S(1)} %all_to_all.10.arrived, ...), custom_call_target="tpu_custom_call" | custom-call | flops 4000000 | bytes 3000000 | tf_op jit(solution)/shard_map/pallas_call | solution.py:538
  45.4 3.6 %all-to-all-done.1 = bf16[128,3,2,128]{3,2,1,0:T(2,128)(2,1)S(1)} async-done(((bf16[128,3,2,128]{3,2,1,0:T(2,128)(2,1)}), bf16[128,3,2,128]{3,2,1,0:T(2,128)(2,1)S(1)}, u32[]{:S(2)}, u32[]{:S(2)}) %all-to-all-start.1) | async-done | bytes 196640 | tf_op jit(solution)/shard_map/all_to_all | solution.py:536
  48.9 0.7 %shard_map.195 = bf16[32,32]{1,0:T(8,128)(2,1)} custom-call(bf16[768,128]{1,0:T(8,128)(2,1)S(1)} %bitcast.11), custom_call_target="tpu_custom_call" | custom-call | tf_op jit(solution)/shard_map/pallas_call | solution.py:558
Async XLA Ops:
  0.6 4.6 %copy-start.2 = (s32[8]{0:T(128)S(1)}, s32[8]{0:T(128)}, u32[]{:S(2)}) copy-start(s32[8]{0:T(128)} %accepted.3) | copy-start | bytes 100
  0.6 4.6 %copy-start = (bf16[64,4096]{1,0:T(8,128)(2,1)S(1)}, bf16[64,4096]{1,0:T(8,128)(2,1)}, u32[]{:S(2)}) copy-start(bf16[64,4096]{1,0:T(8,128)(2,1)} %weight.3) | copy-start | bytes 1572868
  0.7 4.6 %copy-start.3 = (bf16[4,64]{1,0:T(4,128)(2,1)S(1)}, bf16[4,64]{1,0:T(4,128)(2,1)}, u32[]{:S(2)}) copy-start(bf16[4,64]{1,0:T(4,128)(2,1)} %x_kernel.3) | copy-start | bytes 1540
  0.7 4.6 %copy-start.1 = (bf16[8,7,64]{2,0,1:T(8,128)(2,1)S(1)}, bf16[8,7,64]{2,0,1:T(8,128)(2,1)}, u32[]{:S(2)}) copy-start(bf16[8,7,64]{2,0,1:T(8,128)(2,1)} %param.31) | copy-start | bytes 21508
  0.7 4.6 %copy-start.4 = (bf16[64]{0:T(256)(128)(2,1)S(1)}, bf16[64]{0:T(256)(128)(2,1)}, u32[]{:S(2)}) copy-start(bf16[64]{0:T(256)(128)(2,1)} %param.28) | copy-start | bytes 388
  5.4 19.6 %collective-permute-start = (bf16[80,4096]{1,0:T(8,128)(2,1)S(1)}, bf16[80,4096]{1,0:T(8,128)(2,1)S(1)}, u32[]{:S(2)}, u32[]{:S(2)}) collective-permute-start(bf16[80,4096]{1,0:T(8,128)(2,1)S(1)} %get-tuple-element.14), channel_id=1, source_target_pairs={{0,4},{4,0},{1,5},{5,1},{2,6},{6,2},{3,7},{7,3},{8,12},{12,8},{9,1... | collective-permute-start | bytes 1966088 | tf_op jit(solution)/shard_map/ppermute | solution.py:526
  26.8 22.1 %all-to-all-start.1 = ((bf16[128,3,2,128]{3,2,1,0:T(2,128)(2,1)}), bf16[128,3,2,128]{3,2,1,0:T(2,128)(2,1)S(1)}, u32[]{:S(2)}, u32[]{:S(2)}) async-start(bf16[128,3,2,128]{3,2,1,0:T(2,128)(2,1)} %bitcast.15), calls=%async_computation.1 | async-start | bytes 393216 | tf_op jit(solution)/shard_map/all_to_all | solution.py:536

commit v6 on v4

--- a/solution.py
+++ b/solution.py
@@ -23,6 +23,7 @@
 STATE = 128
 LINES = 6
 TILE = (8, 128)
+FAR_ORDER = (11, 0, 1, 2, 3, 4, 5, 6, 7, 8, 9, 10, 12, 13, 14, 15)
 SMALL = 64
 
 F32 = jnp.float32
@@ -253,8 +254,9 @@
         other = jnp.where(second_core, other, turned_half(other))
         return jnp.where(rows_of(own.shape) < HALF, own, other)
 
-    own = summed_over_tp(arrived, pair + core, 0)
-    other = summed_over_tp(arrived, pair + 1 - core, 0)
+    here = pair + 1 - core
+    own = summed_over_tp(arrived, here, 0)
+    other = summed_over_tp(arrived, pair + core, 0)
     got_small = [got[HEAD : HEAD + 16, 128 * i : 128 * i + 128] for i in range(SMALL // 16)]
     small = tiles(kept_pack[0:SMALL, :].astype(F32) + jnp.concatenate(got_small, axis=0).astype(F32))
     gain = swapped(small[0])
@@ -279,8 +281,8 @@
     fresh = [rounded(scale[t] * halves(own[t], other[t])) for t in range(PROPS)]
     sums, extras = [], []
     for g in range(NEAR_KV):
-        sums.append(summed_over_tp(arrived, g, TOKENS))
-        extras.append(tiles(arrived[g * TP + mine, TOKENS : 2 * TOKENS, :].astype(F32)))
+        sums.append(summed_over_tp(arrived, g ^ 1, TOKENS))
+        extras.append(tiles(arrived[(g ^ 1) * TP + mine, TOKENS : 2 * TOKENS, :].astype(F32)))
 
     def terms(left, right):
         window = [jnp.where(lower, swapped(extras[left][m]), extras[right][m]) for m in range(4)]
@@ -323,8 +325,8 @@
     high = rounded(square_line)
     lines = jnp.where(rows % 2 == 0, high, square_line - high)
     copies = []
-    for i in range(weight.shape[1] // 256):
-        cut = slice(256 * i, 256 * (i + 1))
+    for i, eight in enumerate(FAR_ORDER):
+        cut = slice(256 * eight, 256 * (eight + 1))
         both_weights = jnp.concatenate([weight[:, cut], got[0:HEAD, cut]], axis=0)
         product = jnp.dot(turns, both_weights, preferred_element_type=F32)
         pieces = []
@@ -335,7 +337,7 @@
                 spot = None
                 for t in range(PROPS):
                     piece = block[32 * d + 8 * t : 32 * d + 8 * t + 8]
-                    piece = piece if t == d else pltpu.roll(piece, (32 * (t - d)) % 128, 1)
+                    piece = piece if t == d ^ 1 else pltpu.roll(piece, (32 * (t - (d ^ 1))) % 128, 1)
                     spot = piece if t == 0 else jnp.where(quarter == t, piece, spot)
                 spots.append(spot)
             pieces += [
@@ -365,7 +367,7 @@
     bc_window,
     columns,
 ):
-    place = lax.axis_index(("yl", "c"))
+    place = lax.axis_index("yl") * 2 + 1 - lax.axis_index("c")
     mine = lax.axis_index("tp")
     lanes = lanes_of(TILE)
     lower = lanes < HEAD
@@ -381,8 +383,8 @@
         scale.append(column[:, 0:1])
         step.append(softplus(rounded(scale[t] * column[:, 4:5]) + bias))
     fresh = [rounded(scale[t] * own[t]) for t in range(PROPS)]
-    sums = [summed_over_tp(arrived, g, TOKENS) for g in range(2)]
-    extras = [tiles(arrived[g * TP + mine, TOKENS : 2 * TOKENS, :].astype(F32)) for g in range(2)]
+    sums = [summed_over_tp(arrived, g ^ 1, TOKENS) for g in range(2)]
+    extras = [tiles(arrived[(g ^ 1) * TP + mine, TOKENS : 2 * TOKENS, :].astype(F32)) for g in range(2)]
     window = [jnp.where(lower, swapped(extras[0][m]), extras[1][m]) for m in range(4)]
     new = [rounded(scale[t] * jnp.where(lower, sums[0][t], swapped(sums[1][t]))) for t in range(PROPS)]
     b_terms = convolved(window[:3] + new, [window[3][j : j + 1] for j in range(4)])
@@ -416,7 +418,7 @@
     total[...] = running
     sums = []
     for c in range(2):
-        start = LINES * c
+        start = LINES * (1 - c)
         part = total[start : start + LINES, :]
         for i in range(1, 4):
             part = part + total[2 * LINES * i + start : 2 * LINES * i + start + LINES, :]
@@ -500,7 +502,8 @@
     )(accepted, saved_states, hidden, x_weight.T, z_weight.T, bc_weight.T, input_gain, dt_weight.T, bc_rows, bc_kernel)
     first_state = near_memory(first_state)
     output_weight = near_memory(output_weight)
-    arrived = near_memory(lax.all_to_all(near, NEAR, 0, 0, tiled=True))
+    order = [[(g ^ 1) * TP + k for g in range(NEAR_KV) for k in range(TP)]]
+    arrived = near_memory(lax.all_to_all(near, NEAR, 0, 0, tiled=True, axis_index_groups=order))
     kept_pack, sent = pl.pallas_call(
         pack_body,
         out_shape=(held((pack_rows, 128), BF16), held((HEAD + 16, output_weight.shape[1]), BF16)),
@@ -526,7 +529,9 @@
         out_specs=far_memory(),
         scratch_shapes=[pltpu.VMEM((TOKENS, 8), F32), pltpu.VMEM((lines, 128), BF16), pltpu.SemaphoreType.DMA((4,))],
     )(arrived, near_memory(kept_pack), near_memory(got), output_weight)
-    landed = lax.all_to_all(far.reshape(KV_SIZE, LINES // 2, 2, 128), KV, 0, 0, tiled=True)
+    order = [[8 * eight + (i ^ 1) for eight in FAR_ORDER for i in range(8)]]
+    far = far.reshape(KV_SIZE, LINES // 2, 2, 128)
+    landed = lax.all_to_all(far, KV, 0, 0, tiled=True, axis_index_groups=order)
     landed = near_memory(landed.reshape(lines, 128))
     new_states, x_window, bc_window = pl.pallas_call(
         state_body,

time: 55.1 us -> 49 us (0.89)
  waiting for transfers between devices: 11.3 us -> 3.35 us
  starting transfers between devices: 21.8 us -> 23.6 us
    all_to_all x1, waiting for transfers between devices: 11.3 us -> 3.34 us  [local(): landed = lax.all_to_all(far, KV, 0, 0, tiled=True, axis_index_groups=order)]
    all_to_all x1, starting transfers between devices: 13.1 us -> 14.8 us  [local(): landed = lax.all_to_all(far, KV, 0, 0, tiled=True, axis_index_groups=order)]
where the time goes in v6:
time: 49 us; the launch traced here: 48.6 us
  starting transfers between devices  23.6 us (48%)
  blocking collectives  11.2 us (23%)
  Pallas kernels  7.72 us (16%)
  waiting for transfers between devices  3.35 us (7%)
  between operations  2.74 us (6%)
    all_to_all x1, starting transfers between devices, local(): landed = lax.all_to_all(far, KV, 0, 0, tiled=True, axis_index_groups=order)  14.8 us
    all_to_all x1, blocking collectives, local(): lax.all_to_all(near, NEAR, 0, 0, tiled=True, axis_index_groups=order)  11.2 us
    ppermute x1, starting transfers between devices, local(): got = lax.ppermute(sent, 'c', [(0, 1), (1, 0)])  8.74 us
    all_to_all x1, waiting for transfers between devices, local(): landed = lax.all_to_all(far, KV, 0, 0, tiled=True, axis_index_groups=order)  3.34 us
    pallas_call x1, Pallas kernels, local(): pl.pallas_call(state_body, out_shape=(shape((SEQS, PROPS + 1, 1, HEAD, ST...  2.62 us
    pallas_call x1, Pallas kernels, local(): pl.pallas_call(project_body, out_shape=(shape((TP * NEAR_KV, 2 * TOKENS,...  2.55 us
    pallas_call x1, Pallas kernels, local(): pl.pallas_call(mix_body, out_shape=shape((lines, 128), BF16), in_specs=[v...  1.71 us
  transfers between devices with their start and end apart: 2, of which 1 were waited for; matrix products, arithmetic and copies ran while one was open for 0% of the time, Pallas kernels for 5%

profile of v6, /device:TPU:1, one launch (start us, length us, event | category | flops | bytes accessed | tf_op | source)
XLA Modules:
  0.0 48.6 jit_solution(17126781772730767667)
XLA Ops:
  0.6 0.0 copy-start.2
  0.6 0.0 copy-start
  0.7 0.0 copy-start.3
  0.7 0.0 copy-start.1
  0.7 0.0 copy-start.4
  2.7 2.6 %shard_map.192 = (bf16[16,64,128]{2,1,0:T(8,128)(2,1)}, f32[8,64,128]{2,1,0:T(8,128)S(1)}) custom-call(s32[8]{0:T(128)} %accepted.3, f32[8,5,1,64,128]{4,3,2,1,0:T(8,128)} %saved.1, bf16[128,1024]{1,0:T(8,128)(2,1)} %hidden_far.1, bf16[64,1024]{1,0:T(8,128)(2,1)} %bitcast.16, bf16[64,1024]{1,0:T(8,128)(2,1)} %bitcast.17, bf16[64,1024]{1,0:T(8,128)(2,1)} %bitcast.18, ...), custom_call_target="tpu_custom_call" | custom-call | tf_op jit(solution)/shard_map/pallas_call | solution.py:479
  5.2 0.0 copy-done.2
  5.3 0.0 copy-done
  5.3 0.0 copy-done.3
  5.3 0.0 copy-done.1
  5.3 0.0 copy-done.4
  5.3 0.1 shard_map.193
  5.4 8.7 %collective-permute-start = (bf16[80,4096]{1,0:T(8,128)(2,1)S(1)}, bf16[80,4096]{1,0:T(8,128)(2,1)S(1)}, u32[]{:S(2)}, u32[]{:S(2)}) collective-permute-start(bf16[80,4096]{1,0:T(8,128)(2,1)S(1)} %get-tuple-element.14), channel_id=1, source_target_pairs={{0,4},{4,0},{1,5},{5,1},{2,6},{6,2},{3,7},{7,3},{8,12},{12,8},{9,1... | collective-permute-start | bytes 1966088 | tf_op jit(solution)/shard_map/ppermute | solution.py:524
  14.1 11.2 %all_to_all.10.arrived = bf16[16,64,128]{2,1,0:T(8,128)(2,1)S(1)} all-to-all(bf16[16,64,128]{2,1,0:T(8,128)(2,1)} %get-tuple-element.11), channel_id=1, replica_groups={{4,5,6,7,0,1,2,3,12,13,14,15,8,9,10,11},{20,21,22,23,16,17,18,19,28,29,..., dimensions={0} | all-to-all | bytes 524288 | tf_op jit(solution)/shard_map/all_to_all | solution.py:506
  25.3 0.0 collective-permute-done.got
  25.3 1.7 %shard_map.194 = bf16[768,128]{1,0:T(8,128)(2,1)} custom-call(bf16[16,64,128]{2,1,0:T(8,128)(2,1)S(1)} %all_to_all.10.arrived, bf16[320,128]{1,0:T(8,128)(2,1)S(1)} %get-tuple-element.13.kept_pack, bf16[80,4096]{1,0:T(8,128)(2,1)S(1)} %collective-permute-done.got, bf16[64,4096]{1,0:T(8,128)(2,1)S(1)} %copy-done), custom_call_target="tpu_custom_call" | custom-call | tf_op jit(solution)/shard_map/pallas_call | solution.py:525
  27.1 14.8 %all-to-all-start.1 = ((bf16[128,3,2,128]{3,2,1,0:T(2,128)(2,1)}), bf16[128,3,2,128]{3,2,1,0:T(2,128)(2,1)S(1)}, u32[]{:S(2)}, u32[]{:S(2)}) async-start(bf16[128,3,2,128]{3,2,1,0:T(2,128)(2,1)} %bitcast.15), calls=%async_computation.1 | async-start | bytes 393216 | tf_op jit(solution)/shard_map/all_to_all | solution.py:534
  41.9 2.6 %shard_map.196 = (f32[8,5,1,64,128]{4,3,2,1,0:T(8,128)}, bf16[7,8,64]{2,1,0:T(8,128)(2,1)}, bf16[7,8,64]{2,1,0:T(8,128)(2,1)}) custom-call(f32[1]{0:T(128)S(6)} %copy.21.dt_bias, f32[1]{0:T(128)S(6)} %copy.22.decay_log, s32[8]{0:T(128)} %accepted.3, bf16[16,64,128]{2,1,0:T(8,128)(2,1)S(1)} %all_to_all.10.arrived, ...), custom_call_target="tpu_custom_call" | custom-call | flops 4000000 | bytes 3000000 | tf_op jit(solution)/shard_map/pallas_call | solution.py:536
  44.5 3.3 %all-to-all-done.1 = bf16[128,3,2,128]{3,2,1,0:T(2,128)(2,1)S(1)} async-done(((bf16[128,3,2,128]{3,2,1,0:T(2,128)(2,1)}), bf16[128,3,2,128]{3,2,1,0:T(2,128)(2,1)S(1)}, u32[]{:S(2)}, u32[]{:S(2)}) %all-to-all-start.1) | async-done | bytes 196640 | tf_op jit(solution)/shard_map/all_to_all | solution.py:534
  47.9 0.7 %shard_map.195 = bf16[32,32]{1,0:T(8,128)(2,1)} custom-call(bf16[768,128]{1,0:T(8,128)(2,1)S(1)} %bitcast.11), custom_call_target="tpu_custom_call" | custom-call | tf_op jit(solution)/shard_map/pallas_call | solution.py:556
Async XLA Ops:
  0.6 4.6 %copy-start.2 = (s32[8]{0:T(128)S(1)}, s32[8]{0:T(128)}, u32[]{:S(2)}) copy-start(s32[8]{0:T(128)} %accepted.3) | copy-start | bytes 100
  0.6 4.6 %copy-start = (bf16[64,4096]{1,0:T(8,128)(2,1)S(1)}, bf16[64,4096]{1,0:T(8,128)(2,1)}, u32[]{:S(2)}) copy-start(bf16[64,4096]{1,0:T(8,128)(2,1)} %weight.3) | copy-start | bytes 1572868
  0.7 4.6 %copy-start.3 = (bf16[4,64]{1,0:T(4,128)(2,1)S(1)}, bf16[4,64]{1,0:T(4,128)(2,1)}, u32[]{:S(2)}) copy-start(bf16[4,64]{1,0:T(4,128)(2,1)} %x_kernel.3) | copy-start | bytes 1540
  0.7 4.6 %copy-start.1 = (bf16[8,7,64]{2,0,1:T(8,128)(2,1)S(1)}, bf16[8,7,64]{2,0,1:T(8,128)(2,1)}, u32[]{:S(2)}) copy-start(bf16[8,7,64]{2,0,1:T(8,128)(2,1)} %param.31) | copy-start | bytes 21508
  0.7 4.6 %copy-start.4 = (bf16[64]{0:T(256)(128)(2,1)S(1)}, bf16[64]{0:T(256)(128)(2,1)}, u32[]{:S(2)}) copy-start(bf16[64]{0:T(256)(128)(2,1)} %param.28) | copy-start | bytes 388
  5.4 20.0 %collective-permute-start = (bf16[80,4096]{1,0:T(8,128)(2,1)S(1)}, bf16[80,4096]{1,0:T(8,128)(2,1)S(1)}, u32[]{:S(2)}, u32[]{:S(2)}) collective-permute-start(bf16[80,4096]{1,0:T(8,128)(2,1)S(1)} %get-tuple-element.14), channel_id=1, source_target_pairs={{0,4},{4,0},{1,5},{5,1},{2,6},{6,2},{3,7},{7,3},{8,12},{12,8},{9,1... | collective-permute-start | bytes 1966088 | tf_op jit(solution)/shard_map/ppermute | solution.py:524
  27.1 20.8 %all-to-all-start.1 = ((bf16[128,3,2,128]{3,2,1,0:T(2,128)(2,1)}), bf16[128,3,2,128]{3,2,1,0:T(2,128)(2,1)S(1)}, u32[]{:S(2)}, u32[]{:S(2)}) async-start(bf16[128,3,2,128]{3,2,1,0:T(2,128)(2,1)} %bitcast.15), calls=%async_computation.1 | async-start | bytes 393216 | tf_op jit(solution)/shard_map/all_to_all | solution.py:534

commit v7 on v6

--- a/solution.py
+++ b/solution.py
@@ -114,8 +114,10 @@
     dt_weight_far,
     bc_history_far,
     bc_kernel_far,
+    weight_far,
     message,
     first_state,
+    weight,
     chosen,
     accepted,
     hidden,
@@ -149,10 +151,12 @@
     inputs = [pltpu.make_async_copy(a, b, coming.at[i]) for i, (a, b) in enumerate(zip(sources, targets))]
     for copy in inputs:
         copy.start()
+    weight_copy = pltpu.make_async_copy(weight_far, weight, reading.at[SEQS])
     inputs[0].wait()
     reads = [
         pltpu.make_async_copy(saved.at[s, chosen[s], 0], first_state.at[s], reading.at[s]) for s in range(SEQS)
     ]
+    reads.append(weight_copy)
     for copy in reads:
         copy.start()
     for copy in inputs[1:]:
@@ -346,9 +350,9 @@
                 jnp.where((rows >= 2) & (rows < 6), spots[3], lines),
             ]
         block_rows[48 * i : 48 * (i + 1), :] = jnp.concatenate(pieces, axis=0).astype(BF16)
-        if i % 4 == 3:
-            part = pl.ds(48 * (i - 3), 192)
-            copies.append(pltpu.make_async_copy(block_rows.at[part], message.at[part], leaving.at[i // 4]))
+        if i % 2 == 1:
+            part = pl.ds(48 * (i - 1), 96)
+            copies.append(pltpu.make_async_copy(block_rows.at[part], message.at[part], leaving.at[i // 2]))
             copies[-1].start()
     for copy in copies:
         copy.wait()
@@ -476,11 +480,15 @@
     x_rows = jnp.transpose(x_history, (1, 0, 2))
     bc_rows = jnp.transpose(bc_history, (1, 0, 2))
     pack_rows = SMALL + HALF * HEAD
-    near, first_state = pl.pallas_call(
+    near, first_state, output_weight = pl.pallas_call(
         project_body,
-        out_shape=(shape((TP * NEAR_KV, 2 * TOKENS, 128), BF16), held((SEQS, HEAD, STATE), F32)),
-        in_specs=[far_memory()] * 10,
-        out_specs=(far_memory(), vmem()),
+        out_shape=(
+            shape((TP * NEAR_KV, 2 * TOKENS, 128), BF16),
+            held((SEQS, HEAD, STATE), F32),
+            held(output_weight.shape, BF16),
+        ),
+        in_specs=[far_memory()] * 11,
+        out_specs=(far_memory(), vmem(), vmem()),
         scratch_shapes=[
             pltpu.SMEM(accepted.shape, jnp.int32),
             pltpu.VMEM(accepted.shape, jnp.int32),
@@ -496,10 +504,22 @@
             pltpu.VMEM((128, 128), F32),
             pltpu.VMEM((TP, 2 * TOKENS, 128), BF16),
             pltpu.SemaphoreType.DMA((10,)),
-            pltpu.SemaphoreType.DMA((SEQS,)),
+            pltpu.SemaphoreType.DMA((SEQS + 1,)),
             pltpu.SemaphoreType.DMA((TP * NEAR_KV,)),
         ],
-    )(accepted, saved_states, hidden, x_weight.T, z_weight.T, bc_weight.T, input_gain, dt_weight.T, bc_rows, bc_kernel)
+    )(
+        accepted,
+        saved_states,
+        hidden,
+        x_weight.T,
+        z_weight.T,
+        bc_weight.T,
+        input_gain,
+        dt_weight.T,
+        bc_rows,
+        bc_kernel,
+        output_weight,
+    )
     first_state = near_memory(first_state)
     output_weight = near_memory(output_weight)
     order = [[(g ^ 1) * TP + k for g in range(NEAR_KV) for k in range(TP)]]
@@ -527,7 +547,7 @@
         out_shape=shape((lines, 128), BF16),
         in_specs=[vmem()] * 4,
         out_specs=far_memory(),
-        scratch_shapes=[pltpu.VMEM((TOKENS, 8), F32), pltpu.VMEM((lines, 128), BF16), pltpu.SemaphoreType.DMA((4,))],
+        scratch_shapes=[pltpu.VMEM((TOKENS, 8), F32), pltpu.VMEM((lines, 128), BF16), pltpu.SemaphoreType.DMA((8,))],
     )(arrived, near_memory(kept_pack), near_memory(got), output_weight)
     order = [[8 * eight + (i ^ 1) for eight in FAR_ORDER for i in range(8)]]
     far = far.reshape(KV_SIZE, LINES // 2, 2, 128)

time: 49 us -> 49 us (level)
  no operation moved by 1% of the time
where the time goes in v7:
time: 49 us; the launch traced here: 48.6 us
  starting transfers between devices  23.6 us (48%)
  blocking collectives  11.2 us (23%)
  Pallas kernels  7.75 us (16%)
  waiting for transfers between devices  3.35 us (7%)
  between operations  2.7 us (6%)
    all_to_all x1, starting transfers between devices, local(): landed = lax.all_to_all(far, KV, 0, 0, tiled=True, axis_index_groups=order)  14.8 us
    all_to_all x1, blocking collectives, local(): lax.all_to_all(near, NEAR, 0, 0, tiled=True, axis_index_groups=order)  11.2 us
    ppermute x1, starting transfers between devices, local(): got = lax.ppermute(sent, 'c', [(0, 1), (1, 0)])  8.74 us
    all_to_all x1, waiting for transfers between devices, local(): landed = lax.all_to_all(far, KV, 0, 0, tiled=True, axis_index_groups=order)  3.34 us
    pallas_call x1, Pallas kernels, local(): pl.pallas_call(state_body, out_shape=(shape((SEQS, PROPS + 1, 1, HEAD, ST...  2.62 us
    pallas_call x1, Pallas kernels, local(): pl.pallas_call(project_body, out_shape=(shape((TP * NEAR_KV, 2 * TOKENS,...  2.56 us
    pallas_call x1, Pallas kernels, local(): pl.pallas_call(mix_body, out_shape=shape((lines, 128), BF16), in_specs=[v...  1.73 us
  transfers between devices with their start and end apart: 2, of which 1 were waited for; matrix products, arithmetic and copies ran while one was open for 0% of the time, Pallas kernels for 5%

profile of v7, /device:TPU:1, one launch (start us, length us, event | category | flops | bytes accessed | tf_op | source)
XLA Modules:
  0.0 48.6 jit_solution(14501990894579884086)
XLA Ops:
  0.6 0.0 copy-start.1
  0.6 0.0 copy-start.2
  0.7 0.0 copy-start
  0.7 0.0 copy-start.3
  2.6 2.6 %shard_map.192 = (bf16[16,64,128]{2,1,0:T(8,128)(2,1)}, f32[8,64,128]{2,1,0:T(8,128)S(1)}, bf16[64,4096]{1,0:T(8,128)(2,1)S(1)}) custom-call(s32[8]{0:T(128)} %accepted.3, f32[8,5,1,64,128]{4,3,2,1,0:T(8,128)} %saved.1, bf16[128,1024]{1,0:T(8,128)(2,1)} %hidden_far.1, bf16[64,1024]{1,0:T(8,128)(2,1)} %bitcast.16, bf16[64,1024]{1,0:T(8,128)(2,1)} %bitcast.17, ...), custom_call_target="tpu_custom_call" | custom-call | tf_op jit(solution)/shard_map/pallas_call | solution.py:483
  5.2 0.0 copy-done.1
  5.2 0.0 copy-done.2
  5.2 0.0 copy-done
  5.2 0.0 copy-done.3
  5.3 0.1 shard_map.193
  5.3 8.7 %collective-permute-start = (bf16[80,4096]{1,0:T(8,128)(2,1)S(1)}, bf16[80,4096]{1,0:T(8,128)(2,1)S(1)}, u32[]{:S(2)}, u32[]{:S(2)}) collective-permute-start(bf16[80,4096]{1,0:T(8,128)(2,1)S(1)} %get-tuple-element.16), channel_id=1, source_target_pairs={{0,4},{4,0},{1,5},{5,1},{2,6},{6,2},{3,7},{7,3},{8,12},{12,8},{9,1... | collective-permute-start | bytes 1966088 | tf_op jit(solution)/shard_map/ppermute | solution.py:544
  14.1 11.2 %all_to_all.10.arrived = bf16[16,64,128]{2,1,0:T(8,128)(2,1)S(1)} all-to-all(bf16[16,64,128]{2,1,0:T(8,128)(2,1)} %get-tuple-element.12), channel_id=1, replica_groups={{4,5,6,7,0,1,2,3,12,13,14,15,8,9,10,11},{20,21,22,23,16,17,18,19,28,29,..., dimensions={0} | all-to-all | bytes 524288 | tf_op jit(solution)/shard_map/all_to_all | solution.py:526
  25.3 0.0 collective-permute-done.got
  25.3 1.7 %shard_map.194 = bf16[768,128]{1,0:T(8,128)(2,1)} custom-call(bf16[16,64,128]{2,1,0:T(8,128)(2,1)S(1)} %all_to_all.10.arrived, bf16[320,128]{1,0:T(8,128)(2,1)S(1)} %get-tuple-element.15.kept_pack, bf16[80,4096]{1,0:T(8,128)(2,1)S(1)} %collective-permute-done.got, bf16[64,4096]{1,0:T(8,128)(2,1)S(1)} %get-tuple-element.14.weight), custom_call_target="tpu_custom_call" | custom-call | tf_op jit(solution)/shard_map/pallas_call | solution.py:545
  27.0 14.8 %all-to-all-start.1 = ((bf16[128,3,2,128]{3,2,1,0:T(2,128)(2,1)}), bf16[128,3,2,128]{3,2,1,0:T(2,128)(2,1)S(1)}, u32[]{:S(2)}, u32[]{:S(2)}) async-start(bf16[128,3,2,128]{3,2,1,0:T(2,128)(2,1)} %bitcast.15), calls=%async_computation.1 | async-start | bytes 393216 | tf_op jit(solution)/shard_map/all_to_all | solution.py:554
  41.9 2.6 %shard_map.196 = (f32[8,5,1,64,128]{4,3,2,1,0:T(8,128)}, bf16[7,8,64]{2,1,0:T(8,128)(2,1)}, bf16[7,8,64]{2,1,0:T(8,128)(2,1)}) custom-call(f32[1]{0:T(128)S(6)} %copy.21.dt_bias, f32[1]{0:T(128)S(6)} %copy.22.decay_log, s32[8]{0:T(128)} %accepted.3, bf16[16,64,128]{2,1,0:T(8,128)(2,1)S(1)} %all_to_all.10.arrived, ...), custom_call_target="tpu_custom_call" | custom-call | flops 4000000 | bytes 3000000 | tf_op jit(solution)/shard_map/pallas_call | solution.py:556
  44.5 3.3 %all-to-all-done.1 = bf16[128,3,2,128]{3,2,1,0:T(2,128)(2,1)S(1)} async-done(((bf16[128,3,2,128]{3,2,1,0:T(2,128)(2,1)}), bf16[128,3,2,128]{3,2,1,0:T(2,128)(2,1)S(1)}, u32[]{:S(2)}, u32[]{:S(2)}) %all-to-all-start.1) | async-done | bytes 196640 | tf_op jit(solution)/shard_map/all_to_all | solution.py:554
  47.8 0.7 %shard_map.195 = bf16[32,32]{1,0:T(8,128)(2,1)} custom-call(bf16[768,128]{1,0:T(8,128)(2,1)S(1)} %bitcast.11), custom_call_target="tpu_custom_call" | custom-call | tf_op jit(solution)/shard_map/pallas_call | solution.py:576
Async XLA Ops:
  0.6 4.6 %copy-start.1 = (s32[8]{0:T(128)S(1)}, s32[8]{0:T(128)}, u32[]{:S(2)}) copy-start(s32[8]{0:T(128)} %accepted.3) | copy-start | bytes 100
  0.6 4.6 %copy-start.2 = (bf16[4,64]{1,0:T(4,128)(2,1)S(1)}, bf16[4,64]{1,0:T(4,128)(2,1)}, u32[]{:S(2)}) copy-start(bf16[4,64]{1,0:T(4,128)(2,1)} %x_kernel.3) | copy-start | bytes 1540
  0.7 4.6 %copy-start = (bf16[8,7,64]{2,0,1:T(8,128)(2,1)S(1)}, bf16[8,7,64]{2,0,1:T(8,128)(2,1)}, u32[]{:S(2)}) copy-start(bf16[8,7,64]{2,0,1:T(8,128)(2,1)} %param.31) | copy-start | bytes 21508
  0.7 4.6 %copy-start.3 = (bf16[64]{0:T(256)(128)(2,1)S(1)}, bf16[64]{0:T(256)(128)(2,1)}, u32[]{:S(2)}) copy-start(bf16[64]{0:T(256)(128)(2,1)} %param.28) | copy-start | bytes 388
  5.3 20.0 %collective-permute-start = (bf16[80,4096]{1,0:T(8,128)(2,1)S(1)}, bf16[80,4096]{1,0:T(8,128)(2,1)S(1)}, u32[]{:S(2)}, u32[]{:S(2)}) collective-permute-start(bf16[80,4096]{1,0:T(8,128)(2,1)S(1)} %get-tuple-element.16), channel_id=1, source_target_pairs={{0,4},{4,0},{1,5},{5,1},{2,6},{6,2},{3,7},{7,3},{8,12},{12,8},{9,1... | collective-permute-start | bytes 1966088 | tf_op jit(solution)/shard_map/ppermute | solution.py:544
  27.0 20.8 %all-to-all-start.1 = ((bf16[128,3,2,128]{3,2,1,0:T(2,128)(2,1)}), bf16[128,3,2,128]{3,2,1,0:T(2,128)(2,1)S(1)}, u32[]{:S(2)}, u32[]{:S(2)}) async-start(bf16[128,3,2,128]{3,2,1,0:T(2,128)(2,1)} %bitcast.15), calls=%async_computation.1 | async-start | bytes 393216 | tf_op jit(solution)/shard_map/all_to_all | solution.py:554
